TPU v7x, 32 devices: a whole 2x2x4 slice. The times are simulated.
32 devices in a mesh: ep: 8 (over z, x), tp: 4 (over y, core).
Axes of the slice: x: 2, y: 2, z: 4, core: 2. Of those that a mesh axis runs over, the one named last changes fastest.
Arguments:
- tokens: bfloat16 [768, 4096], P('ep'), may hold values from -6 to 6
- mix_gain: float32 [4096], replicated, may hold values from 0.1 to 1.9
- ffn_gain: float32 [4096], replicated, may hold values from 0.1 to 1.9
- in_proj: bfloat16 [4096, 1024], P(None, 'tp'), may hold values from -0.09375 to 0.09375
- decay_rate: float32 [64, 64], P('tp'), may hold values from 0.05 to 2
- frequency: float32 [64, 64], P('tp'), may hold values from -3 to 3
- log_step: float32 [64], P('tp'), may hold values from -3 to 0.5
- b_real: float32 [64, 64, 16], P('tp'), may hold values from -1.5 to 1.5
- b_imag: float32 [64, 64, 16], P('tp'), may hold values from -1.5 to 1.5
- c_real: float32 [64, 16, 64], P('tp'), may hold values from -0.75 to 0.75
- c_imag: float32 [64, 16, 64], P('tp'), may hold values from -0.75 to 0.75
- skip_gain: float32 [1024], P('tp'), may hold values from -5 to 5
- states: float32 [2, 768, 4096], P(None, 'ep', 'tp'), may hold values from -6 to 6
- out_proj: bfloat16 [1024, 4096], P('tp'), may hold values from -0.1875 to 0.1875
- route_ids: int32 [768, 2], P('ep'), may hold values from 0 to 7, all different within a row; in each aligned block of 96 rows (0 to 95, 96 to 191, ...) at most 48 rows name the same one
- route_logits: float32 [768, 2], P('ep'), may hold values from -5 to 5
- expert_gate: bfloat16 [8, 4096, 3072], P('ep', None, 'tp'), may hold values from -0.09375 to 0.09375
- expert_up: bfloat16 [8, 4096, 3072], P('ep', None, 'tp'), may hold values from -0.09375 to 0.09375
- expert_down: bfloat16 [8, 3072, 4096], P('ep', 'tp'), may hold values from -0.109375 to 0.109375
- dense_gate: bfloat16 [4096, 6144], P('tp', 'ep'), may hold values from -0.09375 to 0.09375
- dense_up: bfloat16 [4096, 6144], P('tp', 'ep'), may hold values from -0.09375 to 0.09375
- dense_down: bfloat16 [6144, 4096], P('ep', 'tp'), may hold values from -0.078125 to 0.078125
- branch_gate: bfloat16 [4096], replicated, may hold values from -0.09375 to 0.09375
Outputs:
- output: bfloat16 [768, 4096], P('ep', 'tp')
- new_states: float32 [2, 768, 4096], P(None, 'ep', 'tp')
Inputs may be any that keep to these rules, and one draw needn't show every extreme that they name: `route_ids`: each row names 2 different experts; among the rows of one device (aligned blocks of 96 rows) no expert is named by more than 48 rows.
All inputs are finite; a program needn't handle non-finite values.
Results may differ from a plain program's by a relative error of at most 0.017.
Values may be sent and summed in bfloat16 or wider, within the bound.
A program may use at most 128 MiB of HBM per device.

v0:
```python
import functools
import jax
import jax.numpy as jnp
from jax import lax
from jax.experimental import pallas as pl
from jax.experimental.pallas import tpu as pltpu
from jax.sharding import PartitionSpec as P

GROUP = 16
STATE = 64
MESH = pl.DeviceIdType.MESH


def fast_extent(axis, size):
    if axis == "tp":
        return 2
    extent = 1
    while (2 * extent) * (2 * extent) * 2 <= size:
        extent *= 2
    return extent


class Grid:
    def __init__(self, axis, size):
        self.axis, self.size = axis, size
        self.fast = fast_extent(axis, size)
        self.slow = size // self.fast
        self.me = lax.axis_index(axis)
        self.at_fast = self.me % self.fast
        self.at_slow = self.me // self.fast

    def index(self, slow_step, fast_step):
        slow_at = (self.at_slow + slow_step + self.slow) % self.slow
        fast_at = (self.at_fast + fast_step + self.fast) % self.fast
        return slow_at * self.fast + fast_at

    def peers(self):
        return [self.index(k, 0) for k in range(1, self.slow)] + [
            self.index(0, q) for q in range(1, self.fast)
        ]

    def greet(self):
        barrier = pltpu.get_barrier_semaphore()
        peers = self.peers()
        for peer in peers:
            pl.semaphore_signal(barrier, inc=1, device_id={self.axis: peer}, device_id_type=MESH)
        pl.semaphore_wait(barrier, len(peers))

    def copy(self, source, target, sent, landed, peer):
        return pltpu.make_async_remote_copy(
            src_ref=source,
            dst_ref=target,
            send_sem=sent,
            recv_sem=landed,
            device_id={self.axis: peer},
            device_id_type=MESH,
        )


def part_of(ref, owner, start, rows, width, cols):
    if cols:
        return ref.at[pl.ds(start, rows), pl.ds(pl.multiple_of(owner * width, 128), width)]
    return ref.at[owner, pl.ds(start, rows), :]


def gather_kernel(axis, size, pieces, cols, *refs):
    count = len(pieces)
    ins, outs = refs[:count], refs[count : 2 * count]
    slow_sent, slow_landed, fast_sent, fast_landed, own_sem = refs[2 * count :]
    grid = Grid(axis, size)
    spans = []
    for item, number in enumerate(pieces):
        rows = ins[item].shape[0] // number
        spans += [(item, j, j * rows, rows) for j in range(number)]

    def place(item, owner, start, rows):
        return part_of(outs[item], owner, start, rows, ins[item].shape[1], cols)

    grid.greet()
    pending = []
    for item, j, start, rows in spans:
        for k in range(1, grid.slow):
            copy = grid.copy(
                ins[item].at[pl.ds(start, rows), :],
                place(item, grid.me, start, rows),
                slow_sent.at[item, j, k - 1],
                slow_landed.at[item, j, k - 1],
                grid.index(k, 0),
            )
            copy.start()
            pending.append(copy)
    for item, j, start, rows in spans:
        for q in range(1, grid.fast):
            copy = grid.copy(
                ins[item].at[pl.ds(start, rows), :],
                place(item, grid.me, start, rows),
                fast_sent.at[item, j, 0, q - 1],
                fast_landed.at[item, j, 0, q - 1],
                grid.index(0, q),
            )
            copy.start()
            pending.append(copy)
    owns = []
    for item in range(count):
        own = pltpu.make_async_copy(
            ins[item], place(item, grid.me, 0, ins[item].shape[0]), own_sem.at[item]
        )
        own.start()
        owns.append(own)
    for item, j, start, rows in spans:
        for k in range(1, grid.slow):
            block = place(item, grid.index(-k, 0), start, rows)
            grid.copy(
                block,
                block,
                slow_sent.at[item, j, k - 1],
                slow_landed.at[item, j, k - 1],
                grid.index(-k, 0),
            ).wait_recv()
            for q in range(1, grid.fast):
                copy = grid.copy(
                    block,
                    block,
                    fast_sent.at[item, j, k, q - 1],
                    fast_landed.at[item, j, k, q - 1],
                    grid.index(0, q),
                )
                copy.start()
                pending.append(copy)
    for item, j, start, rows in spans:
        for k in range(grid.slow):
            for q in range(1, grid.fast):
                block = place(item, grid.index(-k, -q), start, rows)
                grid.copy(
                    block,
                    block,
                    fast_sent.at[item, j, k, q - 1],
                    fast_landed.at[item, j, k, q - 1],
                    grid.index(0, -q),
                ).wait_recv()
    for copy in pending:
        copy.wait_send()
    for own in owns:
        own.wait()


def all_gather(arrays, axis, size, pieces, cols, collective_id):
    shapes = []
    for array in arrays:
        rows, width = array.shape
        shape = (rows, size * width) if cols else (size, rows, width)
        shapes.append(jax.ShapeDtypeStruct(shape, array.dtype))
    fast = fast_extent(axis, size)
    slow = size // fast
    count, most = len(arrays), max(pieces)
    sems = [
        pltpu.SemaphoreType.DMA((count, most, slow - 1)),
        pltpu.SemaphoreType.DMA((count, most, slow - 1)),
        pltpu.SemaphoreType.DMA((count, most, slow, fast - 1)),
        pltpu.SemaphoreType.DMA((count, most, slow, fast - 1)),
        pltpu.SemaphoreType.DMA((count,)),
    ]
    return pl.pallas_call(
        functools.partial(gather_kernel, axis, size, pieces, cols),
        out_shape=shapes,
        in_specs=[pl.BlockSpec(memory_space=pltpu.VMEM)] * count,
        out_specs=[pl.BlockSpec(memory_space=pltpu.VMEM)] * count,
        scratch_shapes=sems,
        compiler_params=pltpu.CompilerParams(
            collective_id=collective_id, has_side_effects=True, vmem_limit_bytes=16 << 20
        ),
    )(*arrays)


def reduce_kernel(
    axis,
    size,
    number,
    cols,
    x_ref,
    o_ref,
    got_fast,
    mid,
    got_slow,
    total_ref,
    fast_sent,
    fast_landed,
    slow_sent,
    slow_landed,
):
    grid = Grid(axis, size)
    rows, width = o_ref.shape
    step = rows // number
    grid.greet()
    pending = []
    for k in range(1, grid.slow + 1):
        for j in range(number):
            for q in range(1, grid.fast):
                copy = grid.copy(
                    part_of(x_ref, grid.index(k, q), j * step, step, width, cols),
                    got_fast.at[q - 1, k - 1, pl.ds(j * step, step), :],
                    fast_sent.at[q - 1, k - 1, j],
                    fast_landed.at[q - 1, k - 1, j],
                    grid.index(0, q),
                )
                copy.start()
                pending.append(copy)
    for k in range(1, grid.slow + 1):
        for j in range(number):
            span = pl.ds(j * step, step)
            total = part_of(x_ref, grid.index(k, 0), j * step, step, width, cols)[...].astype(
                jnp.float32
            )
            for q in range(1, grid.fast):
                block = got_fast.at[q - 1, k - 1, span, :]
                grid.copy(
                    block,
                    block,
                    fast_sent.at[q - 1, k - 1, j],
                    fast_landed.at[q - 1, k - 1, j],
                    grid.index(0, -q),
                ).wait_recv()
                total = total + block[...].astype(jnp.float32)
            if k == grid.slow:
                total_ref[span, :] = total
            else:
                mid[k - 1, span, :] = total.astype(mid.dtype)
                copy = grid.copy(
                    mid.at[k - 1, span, :],
                    got_slow.at[k - 1, span, :],
                    slow_sent.at[k - 1, j],
                    slow_landed.at[k - 1, j],
                    grid.index(k, 0),
                )
                copy.start()
                pending.append(copy)
    for j in range(number):
        span = pl.ds(j * step, step)
        total = total_ref[span, :]
        for k in range(1, grid.slow):
            block = got_slow.at[k - 1, span, :]
            grid.copy(
                block,
                block,
                slow_sent.at[k - 1, j],
                slow_landed.at[k - 1, j],
                grid.index(-k, 0),
            ).wait_recv()
            total = total + block[...].astype(jnp.float32)
        o_ref[span, :] = total.astype(o_ref.dtype)
    for copy in pending:
        copy.wait_send()


def reduce_scatter(array, axis, size, number, cols, collective_id):
    if cols:
        rows, width = array.shape[0], array.shape[1] // size
    else:
        rows, width = array.shape[1:]
    fast = fast_extent(axis, size)
    slow = size // fast
    return pl.pallas_call(
        functools.partial(reduce_kernel, axis, size, number, cols),
        out_shape=jax.ShapeDtypeStruct((rows, width), array.dtype),
        in_specs=[pl.BlockSpec(memory_space=pltpu.VMEM)],
        out_specs=pl.BlockSpec(memory_space=pltpu.VMEM),
        scratch_shapes=[
            pltpu.VMEM((fast - 1, slow, rows, width), array.dtype),
            pltpu.VMEM((slow - 1, rows, width), array.dtype),
            pltpu.VMEM((slow - 1, rows, width), array.dtype),
            pltpu.VMEM((rows, width), jnp.float32),
            pltpu.SemaphoreType.DMA((fast - 1, slow, number)),
            pltpu.SemaphoreType.DMA((fast - 1, slow, number)),
            pltpu.SemaphoreType.DMA((slow - 1, number)),
            pltpu.SemaphoreType.DMA((slow - 1, number)),
        ],
        compiler_params=pltpu.CompilerParams(
            collective_id=collective_id, has_side_effects=True, vmem_limit_bytes=24 << 20
        ),
    )(array)

class Gather:
    def __init__(self, grid, source, target, number, cols, sems):
        self.grid, self.source, self.target, self.cols = grid, source, target, cols
        self.slow_sent, self.slow_landed, self.fast_sent, self.fast_landed, self.own_sem = sems
        self.rows, self.width = source.shape
        self.step = self.rows // number
        self.number = number
        self.pending = []

    def place(self, owner, j):
        return part_of(self.target, owner, j * self.step, self.step, self.width, self.cols)

    def slow_copy(self, source, target, j, k, peer):
        return self.grid.copy(
            source, target, self.slow_sent.at[j, k - 1], self.slow_landed.at[j, k - 1], peer
        )

    def fast_copy(self, source, target, j, k, q, peer):
        return self.grid.copy(
            source, target, self.fast_sent.at[j, k, q - 1], self.fast_landed.at[j, k, q - 1], peer
        )

    def launch(self, copy):
        copy.start()
        self.pending.append(copy)

    def start(self):
        grid = self.grid
        for j in range(self.number):
            piece = self.source.at[pl.ds(j * self.step, self.step), :]
            spot = self.place(grid.me, j)
            for k in range(1, grid.slow):
                self.launch(self.slow_copy(piece, spot, j, k, grid.index(k, 0)))
        for j in range(self.number):
            piece = self.source.at[pl.ds(j * self.step, self.step), :]
            spot = self.place(grid.me, j)
            for q in range(1, grid.fast):
                self.launch(self.fast_copy(piece, spot, j, 0, q, grid.index(0, q)))
        self.own = pltpu.make_async_copy(
            self.source,
            part_of(self.target, grid.me, 0, self.rows, self.width, self.cols),
            self.own_sem,
        )
        self.own.start()

    def relay(self):
        grid = self.grid
        for j in range(self.number):
            for k in range(1, grid.slow):
                spot = self.place(grid.index(-k, 0), j)
                self.slow_copy(spot, spot, j, k, grid.index(-k, 0)).wait_recv()
                for q in range(1, grid.fast):
                    self.launch(self.fast_copy(spot, spot, j, k, q, grid.index(0, q)))

    def arrive(self):
        grid = self.grid
        for j in range(self.number):
            for k in range(grid.slow):
                for q in range(1, grid.fast):
                    spot = self.place(grid.index(-k, -q), j)
                    self.fast_copy(spot, spot, j, k, q, grid.index(0, -q)).wait_recv()
        self.own.wait()

    def finish(self):
        for copy in self.pending:
            copy.wait_send()


def gather_sems(grid_fast, grid_slow, number):
    return [
        pltpu.SemaphoreType.DMA((number, grid_slow - 1)),
        pltpu.SemaphoreType.DMA((number, grid_slow - 1)),
        pltpu.SemaphoreType.DMA((number, grid_slow, grid_fast - 1)),
        pltpu.SemaphoreType.DMA((number, grid_slow, grid_fast - 1)),
        pltpu.SemaphoreType.DMA,
    ]


class Reduce:
    def __init__(self, grid, source, number, cols, scratch):
        self.grid, self.source, self.cols, self.number = grid, source, cols, number
        self.got_fast, self.mid, self.got_slow, self.total = scratch[:4]
        self.fast_sent, self.fast_landed, self.slow_sent, self.slow_landed = scratch[4:]
        rows, self.width = self.total.shape
        self.step = rows // number
        self.pending = []

    def part(self, dest, j):
        return part_of(self.source, dest, j * self.step, self.step, self.width, self.cols)

    def span(self, j):
        return pl.ds(j * self.step, self.step)

    def fast_copy(self, source, k, j, q, peer):
        return self.grid.copy(
            source,
            self.got_fast.at[q - 1, k - 1, self.span(j), :],
            self.fast_sent.at[q - 1, k - 1, j],
            self.fast_landed.at[q - 1, k - 1, j],
            peer,
        )

    def slow_copy(self, k, j, peer):
        return self.grid.copy(
            self.mid.at[k - 1, self.span(j), :],
            self.got_slow.at[k - 1, self.span(j), :],
            self.slow_sent.at[k - 1, j],
            self.slow_landed.at[k - 1, j],
            peer,
        )

    def push(self):
        grid = self.grid
        for k in range(1, grid.slow + 1):
            for j in range(self.number):
                for q in range(1, grid.fast):
                    copy = self.fast_copy(
                        self.part(grid.index(k, q), j), k, j, q, grid.index(0, q)
                    )
                    copy.start()
                    self.pending.append(copy)

    def relay(self):
        grid = self.grid
        for k in range(1, grid.slow + 1):
            for j in range(self.number):
                value = self.part(grid.index(k, 0), j)[...].astype(jnp.float32)
                for q in range(1, grid.fast):
                    block = self.got_fast.at[q - 1, k - 1, self.span(j), :]
                    self.fast_copy(block, k, j, q, grid.index(0, -q)).wait_recv()
                    value = value + block[...].astype(jnp.float32)
                if k == grid.slow:
                    self.total[self.span(j), :] = value
                else:
                    self.mid[k - 1, self.span(j), :] = value.astype(self.mid.dtype)
                    copy = self.slow_copy(k, j, grid.index(k, 0))
                    copy.start()
                    self.pending.append(copy)

    def collect(self, emit):
        grid = self.grid
        for j in range(self.number):
            value = self.total[self.span(j), :]
            for k in range(1, grid.slow):
                self.slow_copy(k, j, grid.index(-k, 0)).wait_recv()
                value = value + self.got_slow[k - 1, self.span(j), :].astype(jnp.float32)
            emit(self.span(j), value)

    def finish(self):
        for copy in self.pending:
            copy.wait_send()


def reduce_scratch(fast, slow, rows, width, number):
    return [
        pltpu.VMEM((fast - 1, slow, rows, width), jnp.bfloat16),
        pltpu.VMEM((slow - 1, rows, width), jnp.bfloat16),
        pltpu.VMEM((slow - 1, rows, width), jnp.bfloat16),
        pltpu.VMEM((rows, width), jnp.float32),
        pltpu.SemaphoreType.DMA((fast - 1, slow, number)),
        pltpu.SemaphoreType.DMA((fast - 1, slow, number)),
        pltpu.SemaphoreType.DMA((slow - 1, number)),
        pltpu.SemaphoreType.DMA((slow - 1, number)),
    ]


def tile_of(extent):
    for tile in (256, 128):
        if extent % tile == 0:
            return tile
    return extent


def branches_kernel(
    axis,
    size,
    rows_ref,
    cols_ref,
    dense_gate,
    dense_up,
    gate_hbm,
    up_hbm,
    down_hbm,
    dense_out,
    expert_out,
    full,
    gate,
    up,
    down,
    both,
    own_hidden,
    hidden,
    part,
    weight_sems,
    *rest,
):
    grid = Grid(axis, size)
    rows_gather = Gather(grid, rows_ref, full, ROW_PIECES, True, rest[:5])
    hidden_gather = Gather(grid, own_hidden, dense_out, 2, False, rest[5:10])
    dense_sum = Reduce(grid, both, 4, False, rest[10:18])
    expert_sum = Reduce(grid, part, 4, True, rest[18:26])
    loads = []
    for item, (source, target) in enumerate(((gate_hbm, gate), (up_hbm, up), (down_hbm, down))):
        load = pltpu.make_async_copy(source, target, weight_sems.at[item])
        load.start()
        loads.append(load)
    grid.greet()
    rows_gather.start()
    share, double = both.shape[1:]
    width = double // 2

    @pl.loop(0, size)
    def _(dest):
        start = pl.multiple_of(dest * share, 16)
        block = cols_ref[pl.ds(start, share), :]
        both[dest, :, :width] = jnp.dot(
            block, dense_gate[...], preferred_element_type=jnp.float32
        ).astype(jnp.bfloat16)
        both[dest, :, width:] = jnp.dot(
            block, dense_up[...], preferred_element_type=jnp.float32
        ).astype(jnp.bfloat16)

    dense_sum.push()
    dense_sum.relay()
    rows_gather.relay()
    rows_gather.arrive()
    loads[0].wait()
    loads[1].wait()
    inner = hidden.shape[1]
    tile = tile_of(inner)

    @pl.loop(0, inner // tile)
    def _(step):
        span = pl.ds(pl.multiple_of(step * tile, 128), tile)
        gate_val = jnp.dot(full[...], gate[:, span], preferred_element_type=jnp.float32)
        up_val = jnp.dot(full[...], up[:, span], preferred_element_type=jnp.float32)
        hidden[:, span] = (jax.nn.silu(gate_val) * up_val).astype(jnp.bfloat16)

    def emit_hidden(span, value):
        own_hidden[span, :] = (jax.nn.silu(value[:, :width]) * value[:, width:]).astype(
            jnp.bfloat16
        )

    dense_sum.collect(emit_hidden)
    loads[2].wait()
    hidden_gather.start()
    wide = 2 * tile_of(part.shape[1])

    @pl.loop(0, part.shape[1] // wide)
    def _(step):
        span = pl.ds(pl.multiple_of(step * wide, 128), wide)
        part[:, span] = jnp.dot(
            hidden[...], down[:, span], preferred_element_type=jnp.float32
        ).astype(jnp.bfloat16)

    expert_sum.push()
    expert_sum.relay()
    hidden_gather.relay()
    hidden_gather.arrive()

    def emit_expert(span, value):
        expert_out[span, :] = value.astype(expert_out.dtype)

    expert_sum.collect(emit_expert)
    for phase in (rows_gather, hidden_gather, dense_sum, expert_sum):
        phase.finish()


ROW_PIECES = 4


def branches(rows, every_cols, dense_gate, dense_up, gate, up, down, axis, size, collective_id):
    room, width = rows.shape
    total, hidden_width = every_cols.shape[0], dense_gate.shape[1]
    share, inner = total // size, gate.shape[1]
    fast = fast_extent(axis, size)
    slow = size // fast
    whole = pl.BlockSpec(memory_space=pltpu.VMEM)
    far = pl.BlockSpec(memory_space=pl.ANY)
    bf16 = jnp.bfloat16
    return pl.pallas_call(
        functools.partial(branches_kernel, axis, size),
        out_shape=(
            jax.ShapeDtypeStruct((size, share, hidden_width), bf16),
            jax.ShapeDtypeStruct((room, width), bf16),
        ),
        in_specs=[whole] * 4 + [far] * 3,
        out_specs=(whole, whole),
        scratch_shapes=[
            pltpu.VMEM((room, size * width), bf16),
            pltpu.VMEM(gate.shape, bf16),
            pltpu.VMEM(up.shape, bf16),
            pltpu.VMEM(down.shape, bf16),
            pltpu.VMEM((size, share, 2 * hidden_width), bf16),
            pltpu.VMEM((share, hidden_width), bf16),
            pltpu.VMEM((room, inner), bf16),
            pltpu.VMEM((room, size * width), bf16),
            pltpu.SemaphoreType.DMA((3,)),
        ]
        + gather_sems(fast, slow, ROW_PIECES)
        + gather_sems(fast, slow, 2)
        + reduce_scratch(fast, slow, share, 2 * hidden_width, 4)
        + reduce_scratch(fast, slow, room, width, 4),
        compiler_params=pltpu.CompilerParams(
            collective_id=collective_id, has_side_effects=True, vmem_limit_bytes=54 << 20
        ),
    )(rows, every_cols, dense_gate, dense_up, gate, up, down)


def rms_norm(values, gain):
    flt = values.astype(jnp.float32)
    scaled = flt * lax.rsqrt(jnp.mean(flt * flt, axis=-1, keepdims=True) + 1e-06)
    return (scaled * gain).astype(jnp.bfloat16)


def discretize(decay_rate, frequency, log_step, b_real, b_imag):
    step_size = jnp.exp(log_step)[:, None]
    lam_re = -decay_rate
    magnitude = jnp.exp(lam_re * step_size)
    abar_re = magnitude * jnp.cos(frequency * step_size)
    abar_im = magnitude * jnp.sin(frequency * step_size)
    denom = lam_re * lam_re + frequency * frequency
    fac_re = ((abar_re - 1.0) * lam_re + abar_im * frequency) / denom
    fac_im = (abar_im * lam_re - (abar_re - 1.0) * frequency) / denom
    bbar_re = fac_re[..., None] * b_real - fac_im[..., None] * b_imag
    bbar_im = fac_re[..., None] * b_imag + fac_im[..., None] * b_real
    return (abar_re, abar_im, bbar_re, bbar_im)


def state_step(
    drive, states, decay_rate, frequency, log_step, b_real, b_imag, c_real, c_imag, skip_gain
):
    count = drive.shape[0]
    groups = decay_rate.shape[0]
    abar_re, abar_im, bbar_re, bbar_im = discretize(decay_rate, frequency, log_step, b_real, b_imag)
    grouped = drive.astype(jnp.float32).reshape(count, groups, GROUP)
    old_re = states[0].reshape(count, groups, STATE)
    old_im = states[1].reshape(count, groups, STATE)
    high = lax.Precision.HIGHEST
    push_re = jnp.einsum("ngh,gph->ngp", grouped, bbar_re, precision=high)
    push_im = jnp.einsum("ngh,gph->ngp", grouped, bbar_im, precision=high)
    new_re = abar_re * old_re - abar_im * old_im + push_re
    new_im = abar_re * old_im + abar_im * old_re + push_im
    readout = (
        jnp.einsum("ngp,ghp->ngh", new_re, c_real, precision=high)
        - jnp.einsum("ngp,ghp->ngh", new_im, c_imag, precision=high)
        + skip_gain.reshape(groups, GROUP) * grouped
    )
    reads = jax.nn.gelu(readout.reshape(count, groups * GROUP)).astype(jnp.bfloat16)
    fresh = jnp.stack(
        [new_re.reshape(count, groups * STATE), new_im.reshape(count, groups * STATE)]
    )
    return (reads, fresh)


def shards(
    tokens,
    mix_gain,
    ffn_gain,
    in_proj,
    decay_rate,
    frequency,
    log_step,
    b_real,
    b_imag,
    c_real,
    c_imag,
    skip_gain,
    states,
    out_proj,
    route_ids,
    route_logits,
    expert_gate,
    expert_up,
    expert_down,
    dense_gate,
    dense_up,
    dense_down,
    branch_gate,
):
    seq_count, width = tokens.shape
    tp_count = lax.axis_size("tp")
    ep_count = lax.axis_size("ep")
    tp_index = lax.axis_index("tp")
    part_width = width // tp_count
    normed = rms_norm(tokens, mix_gain)
    drive = jnp.dot(normed, in_proj, preferred_element_type=jnp.float32).astype(jnp.bfloat16)
    reads, new_states = state_step(
        drive, states, decay_rate, frequency, log_step, b_real, b_imag, c_real, c_imag, skip_gain
    )
    partial_value = (
        jnp.dot(reads, out_proj, preferred_element_type=jnp.float32)
        .astype(jnp.bfloat16)
        .astype(jnp.float32)
    )
    mixed_cols = reduce_scatter(partial_value.astype(jnp.bfloat16), "tp", tp_count, 2, True, 0)
    (mixed,) = all_gather([mixed_cols], "tp", tp_count, [2], True, 1)
    resid = (tokens.astype(jnp.float32) + mixed.astype(jnp.float32)).astype(jnp.bfloat16)
    normed_two = rms_norm(resid, ffn_gain)
    own_cols = lax.dynamic_slice_in_dim(normed_two, tp_index * part_width, part_width, 1)
    branch = jax.nn.sigmoid(jnp.dot(normed_two, branch_gate, preferred_element_type=jnp.float32))
    route_weights = jax.nn.softmax(route_logits, axis=-1)
    top_count = route_ids.shape[1]
    side = jnp.concatenate(
        [route_ids.astype(jnp.float32).T, route_weights.T, branch[None, :]], axis=0
    )
    side = jnp.pad(side, ((0, -side.shape[0] % 8), (0, -seq_count % 128)))
    every_cols, every_side = all_gather([own_cols, side], "ep", ep_count, [2, 1], False, 2)
    total_count = ep_count * seq_count
    every_cols = every_cols.reshape(total_count, part_width)
    every_side = every_side[:, :, :seq_count].transpose(1, 0, 2).reshape(-1, total_count)
    every_ids = every_side[:top_count].T
    every_weights = every_side[top_count : 2 * top_count].T
    every_branch = every_side[2 * top_count]
    mine = every_ids == lax.axis_index("ep").astype(jnp.float32)
    taken = jnp.any(mine, axis=1)
    own_weight = jnp.sum(jnp.where(mine, every_weights, 0.0), axis=1)
    order = jnp.cumsum(taken.astype(jnp.int32)) - 1
    room = ep_count * max(2, 2 * seq_count * top_count // ep_count)
    slots = jnp.arange(room, dtype=jnp.int32)
    select = (order[None, :] == slots[:, None]) & taken[None, :]
    row_weight = jnp.sum(jnp.where(select, own_weight[None, :], 0.0), axis=1)
    select = select.astype(jnp.bfloat16)
    expert_in = jnp.dot(select, every_cols, preferred_element_type=jnp.float32).astype(jnp.bfloat16)
    dense_hidden, expert_cols = branches(
        expert_in,
        every_cols,
        dense_gate,
        dense_up,
        expert_gate[0],
        expert_up[0],
        expert_down[0],
        "tp",
        tp_count,
        3,
    )
    dense_hidden = dense_hidden.reshape(total_count, dense_gate.shape[1])
    weighted = (expert_cols.astype(jnp.float32) * row_weight[:, None]).astype(jnp.bfloat16)
    routed_part = lax.dot_general(
        select, weighted, (((0,), (0,)), ((), ())), preferred_element_type=jnp.float32
    )
    dense_part = jnp.dot(dense_hidden, dense_down, preferred_element_type=jnp.float32)
    share = (routed_part + every_branch[:, None] * dense_part).astype(jnp.bfloat16)
    share = share.reshape(ep_count, seq_count, part_width)
    gathered = reduce_scatter(share, "ep", ep_count, 2, False, 4)
    resid_cols = lax.dynamic_slice_in_dim(resid, tp_index * part_width, part_width, 1)
    output = (resid_cols.astype(jnp.float32) + gathered.astype(jnp.float32)).astype(jnp.bfloat16)
    return (output, new_states)


def solution(mesh):
    return jax.shard_map(
        shards,
        mesh=mesh,
        in_specs=(
            P("ep", None),
            P(),
            P(),
            P(None, "tp"),
            P("tp", None),
            P("tp", None),
            P("tp"),
            P("tp", None, None),
            P("tp", None, None),
            P("tp", None, None),
            P("tp", None, None),
            P("tp"),
            P(None, "ep", "tp"),
            P("tp", None),
            P("ep", None),
            P("ep", None),
            P("ep", None, "tp"),
            P("ep", None, "tp"),
            P("ep", "tp", None),
            P("tp", "ep"),
            P("tp", "ep"),
            P("ep", "tp"),
            P(),
        ),
        out_specs=(P("ep", "tp"), P(None, "ep", "tp")),
        check_vma=False,
    )
```

profile of v0, /device:TPU:0, one launch (start us, length us, event | category | flops | bytes accessed | tf_op | source)
XLA Modules:
  0.0 164.1 jit_solution(2018472023410874437)
XLA Ops:
  0.6 0.0 copy-start
  0.7 0.8 reduce_max.9
  1.5 0.7 fusion.47
  2.2 1.3 divide_bitcast_fusion
  3.5 0.7 exp.12
  4.1 1.4 fusion.3
  5.5 1.2 convert_bitcast_fusion
  6.8 0.8 mul.217
  7.5 0.7 reshape.99
  8.2 0.8 add_divide_fusion
  9.1 2.4 %convolution_convert_fusion.2 = bf16[96,256]{1,0:T(8,128)(2,1)S(1)} fusion(bf16[4096,256]{1,0:T(8,128)(2,1)} %param.26, bf16[96,4096]{1,0:T(8,128)(2,1)} %param.23, f32[4096]{0:T(1024)} %param.24, f32[96]{0:T(128)S(1)} %add_rsqrt_fusion.1), kind=kOutput, calls=%fused_computation.27 | convolution fusion | flops 202924032 | bytes 2949504 | tf_op jit(solution)/shard_map/dot_general | solution.py:668
  11.5 0.1 copy.39
  11.6 1.2 fusion.50
  12.8 0.2 copy.37
  13.0 0.0 copy-start.2
  13.0 0.0 copy-start.5
  13.0 0.0 copy-start.6
  13.0 1.0 copy.38
  14.0 0.0 copy-done.2
  14.0 2.0 %fusion.7 = f32[96,16,64]{0,2,1:T(8,128)S(1)} fusion(bf16[96,16,16]{0,2,1:T(8,128)(2,1)S(1)} %bitcast.73, f32[96,16,64]{0,2,1:T(8,128)S(1)} %bitcast.69, f32[96,16,64]{0,2,1:T(8,128)} %bitcast.71, f32[16,64]{1,0:T(8,128)S(1)} %get-tuple-element.17, f32[16,64]{1,0:T(8,128)S(1)} %get-tuple-element.15, f32[16,64,16]{1,2,0:T(8,128)} %param.30, ...), kind=kOutput, calls=%fused_computation.17 | convolution fusion | flops 19316736 | bytes 1376256 | tf_op jit(solution)/shard_map/ngh,gph->ngp/dot_general | solution.py:622
  16.0 0.0 copy-done.5
  16.0 0.0 copy-done.6
  16.0 0.0 copy-done.3
  16.1 0.0 copy-start.8
  16.1 1.9 %fusion.8 = f32[96,16,64]{0,2,1:T(8,128)S(1)} fusion(bf16[96,16,16]{0,2,1:T(8,128)(2,1)S(1)} %bitcast.74, f32[96,16,64]{0,2,1:T(8,128)S(1)} %bitcast.72, f32[96,16,64]{0,2,1:T(8,128)} %bitcast.70, f32[16,64]{1,0:T(8,128)S(1)} %get-tuple-element.17, f32[16,64]{1,0:T(8,128)S(1)} %get-tuple-element.15, f32[16,64,16]{1,2,0:T(8,128)S(1)} %copy-done.5, ...), kind=kOutput, calls=%fused_computation.19 | convolution fusion | flops 19316736 | bytes 1376256 | tf_op jit(solution)/shard_map/ngh,gph->ngp/dot_general | solution.py:621
  17.9 0.0 copy-done.9
  17.9 0.6 fusion.51
  18.5 0.0 copy-done.8
  18.5 0.6 fusion.14
  19.1 0.7 fusion.35
  19.8 0.2 copy.41
  20.0 0.0 copy-start.7
  20.0 0.2 copy.40
  20.2 0.9 pad_maximum_fusion
  21.1 0.0 copy-done
  21.1 0.0 copy-done.7
  21.1 0.5 convolution_convert_fusion.x_ref
  21.6 0.0 copy-start.4
  21.6 9.6 %shard_map.230.refs_0_ = bf16[96,1024]{1,0:T(8,128)(2,1)S(1)} custom-call(bf16[96,4096]{1,0:T(8,128)(2,1)S(1)} %convolution_convert_fusion.x_ref), custom_call_target="tpu_custom_call" | custom-call | tf_op jit(solution)/shard_map/pallas_call | solution.py:262
  31.2 0.0 copy-start.10
  31.2 8.2 %shard_map.231 = bf16[96,4096]{1,0:T(8,128)(2,1)S(1)} custom-call(bf16[96,1024]{1,0:T(8,128)(2,1)S(1)} %shard_map.230.refs_0_), custom_call_target="tpu_custom_call" | custom-call | tf_op jit(solution)/shard_map/pallas_call | solution.py:163
  39.4 0.4 fusion
  39.8 0.3 fusion.2
  40.1 0.3 fusion.19
  40.4 0.0 copy-done.11
  40.5 27.7 %shard_map.232 = (bf16[8,96,1024]{2,1,0:T(8,128)(2,1)S(1)}, f32[8,8,128]{2,1,0:T(8,128)S(1)}) custom-call(bf16[96,1024]{1,0:T(8,128)(2,1)S(1)} %constant_dynamic-slice_fusion.refs_0_, f32[8,128]{1,0:T(8,128)S(1)} %select_maximum_fusion.refs_1_), custom_call_target="tpu_custom_call" | custom-call | tf_op jit(solution)/shard_map/pallas_call | solution.py:163
  68.2 1.1 copy-done.1
  69.4 0.1 reduce_or.12
  69.5 0.1 reshape.98
  69.6 0.3 reduce-window.9
  69.9 0.1 mul.235
  70.0 0.1 reduce_sum.51
  70.0 0.1 slice.32
  70.1 0.1 slice_reduce_fusion.1
  70.3 0.1 add_bitcast_fusion
  70.3 0.3 select_reduce_fusion
  70.7 3.1 %convolution_convert_fusion.1.rows_ref = bf16[384,1024]{1,0:T(8,128)(2,1)} fusion(bf16[768,1024]{1,0:T(8,128)(2,1)} %bitcast.61, s32[768]{0:T(1024)S(1)} %add_bitcast_fusion, pred[768]{0:T(1024)(128)(4,1)S(1)} %reduce_or.12), kind=kOutput, calls=%fused_computation.15 | convolution fusion | flops 604962816 | bytes 2363136 | tf_op jit(solution)/shard_map/dot_general | solution.py:705
  73.7 60.2 %shard_map.233 = (bf16[4,192,768]{2,1,0:T(8,128)(2,1)}, bf16[384,1024]{1,0:T(8,128)(2,1)}) custom-call(bf16[384,1024]{1,0:T(8,128)(2,1)} %convolution_convert_fusion.1.rows_ref, bf16[768,1024]{1,0:T(8,128)(2,1)} %bitcast.62, bf16[1024,768]{1,0:T(8,128)(2,1)} %dense_gate.1, bf16[1024,768]{1,0:T(8,128)(2,1)} %dense_up.1, bf16[4096,768]{1,0:T(8,128)(2,1)} %bitcast.64, ...), custom_call_target="tpu_custom_call" | custom-call | tf_op jit(solution)/shard_map/pallas_call | solution.py:562
  133.9 0.0 copy-start.13
  133.9 0.0 copy-start.14
  133.9 2.4 %fusion.10 = f32[768,1024]{1,0:T(8,128)S(1)} fusion(bf16[384,1024]{1,0:T(8,128)(2,1)} %get-tuple-element.8, f32[384]{0:T(512)S(1)} %select_reduce_fusion, s32[768]{0:T(1024)S(1)} %add_bitcast_fusion, pred[768]{0:T(1024)(128)(4,1)S(1)} %reduce_or.12), kind=kOutput, calls=%fused_computation.23 | convolution fusion | flops 605749248 | bytes 3937536 | tf_op jit(solution)/shard_map/dot_general | solution.py:720
  136.4 1.4 add_convert_fusion
  137.8 25.6 %shard_map.234 = bf16[96,1024]{1,0:T(8,128)(2,1)S(1)} custom-call(bf16[8,96,1024]{2,1,0:T(8,128)(2,1)S(1)} %bitcast.63), custom_call_target="tpu_custom_call" | custom-call | tf_op jit(solution)/shard_map/pallas_call | solution.py:262
  163.3 0.7 add_convert_fusion.1
  (20 shorter events, 0.2 us)
Async XLA Ops:
  0.6 20.5 %copy-start = (bf16[256,4096]{1,0:T(8,128)(2,1)S(1)}, bf16[256,4096]{1,0:T(8,128)(2,1)}, u32[]{:S(2)}) copy-start(bf16[256,4096]{1,0:T(8,128)(2,1)} %param.36) | copy-start | bytes 6291460
  13.0 1.0 copy-start.2
  13.0 3.1 %copy-start.5 = (f32[16,64,16]{1,2,0:T(8,128)S(1)}, f32[16,64,16]{1,2,0:T(8,128)}, u32[]{:S(2)}) copy-start(f32[16,64,16]{1,2,0:T(8,128)} %param.31) | copy-start | bytes 196612
  13.0 3.1 %copy-start.6 = (f32[16,64,16]{1,2,0:T(8,128)S(1)}, f32[16,64,16]{1,2,0:T(8,128)}, u32[]{:S(2)}) copy-start(f32[16,64,16]{1,2,0:T(8,128)} %param.30) | copy-start | bytes 196612
  14.0 2.1 %copy-start.3 = (f32[1,96,1024]{1,2,0:T(8,128)S(1)}, f32[1,96,1024]{1,2,0:T(8,128)}, u32[]{:S(2)}) copy-start(f32[1,96,1024]{1,2,0:T(8,128)} %copy.38) | copy-start | bytes 1179652
  14.0 3.9 %copy-start.9 = (f32[16,16,64]{2,1,0:T(8,128)S(1)}, f32[16,16,64]{2,1,0:T(8,128)}, u32[]{:S(2)}) copy-start(f32[16,16,64]{2,1,0:T(8,128)} %param.32) | copy-start | bytes 196612
  16.1 2.5 %copy-start.8 = (f32[16,16,64]{2,1,0:T(8,128)S(1)}, f32[16,16,64]{2,1,0:T(8,128)}, u32[]{:S(2)}) copy-start(f32[16,16,64]{2,1,0:T(8,128)} %param.33) | copy-start | bytes 196612
  20.0 1.1 copy-start.7
  21.6 17.8 %copy-start.4 = (bf16[96,4096]{1,0:T(8,128)(2,1)S(1)}, bf16[96,4096]{1,0:T(8,128)(2,1)}, u32[]{:S(2)}) copy-start(bf16[96,4096]{1,0:T(8,128)(2,1)} %param.23) | copy-start | bytes 2359300
  31.2 8.6 %copy-start.10 = (f32[4096]{0:T(1024)S(1)}, f32[4096]{0:T(1024)}, u32[]{:S(2)}) copy-start(f32[4096]{0:T(1024)} %param.25) | copy-start | bytes 49156
  39.8 0.7 copy-start.11
  39.8 0.7 copy-start.12
  68.2 1.2 copy-start.1
  133.9 2.4 %copy-start.13 = (bf16[768,1024]{1,0:T(8,128)(2,1)S(1)}, bf16[768,1024]{1,0:T(8,128)(2,1)}, u32[]{:S(2)}) copy-start(bf16[768,1024]{1,0:T(8,128)(2,1)} %param.44) | copy-start | bytes 4718596
  133.9 2.4 %copy-start.14 = (bf16[4,192,768]{2,1,0:T(8,128)(2,1)S(1)}, bf16[4,192,768]{2,1,0:T(8,128)(2,1)}, u32[]{:S(2)}) copy-start(bf16[4,192,768]{2,1,0:T(8,128)(2,1)} %get-tuple-element.9) | copy-start | bytes 3538948
where the time goes:
time: 165 us; the launch traced here: 164 us
  Pallas kernels  131 us (79%)
  matrix products  15.1 us (9%)
  other arithmetic  10 us (6%)
  local copies, waits for them, and re-layouts  6.79 us (4%)
    pallas_call x1, Pallas kernels, branches(): pl.pallas_call(functools.partial(branches_kernel, axis, size), out_shape=...  60.2 us
    pallas_call x2, Pallas kernels, all_gather(): pl.pallas_call(functools.partial(gather_kernel, axis, size, pieces, cols)...  35.9 us
    pallas_call x2, Pallas kernels, reduce_scatter(): pl.pallas_call(functools.partial(reduce_kernel, axis, size, number, cols)...  35.1 us

commit v1 on v0

--- a/solution.py
+++ b/solution.py
@@ -45,6 +45,17 @@
         for peer in peers:
             pl.semaphore_signal(barrier, inc=1, device_id={self.axis: peer}, device_id_type=MESH)
         pl.semaphore_wait(barrier, len(peers))
+
+    def greet_all(self):
+        barrier = pltpu.get_barrier_semaphore()
+        for k in range(1, self.size):
+            pl.semaphore_signal(
+                barrier,
+                inc=1,
+                device_id={self.axis: (self.me + k) % self.size},
+                device_id_type=MESH,
+            )
+        pl.semaphore_wait(barrier, self.size - 1)
 
     def copy(self, source, target, sent, landed, peer):
         return pltpu.make_async_remote_copy(
@@ -390,16 +401,17 @@
             peer,
         )
 
+    def push_part(self, k, q):
+        grid = self.grid
+        for j in range(self.number):
+            copy = self.fast_copy(self.part(grid.index(k, q), j), k, j, q, grid.index(0, q))
+            copy.start()
+            self.pending.append(copy)
+
     def push(self):
-        grid = self.grid
-        for k in range(1, grid.slow + 1):
-            for j in range(self.number):
-                for q in range(1, grid.fast):
-                    copy = self.fast_copy(
-                        self.part(grid.index(k, q), j), k, j, q, grid.index(0, q)
-                    )
-                    copy.start()
-                    self.pending.append(copy)
+        for k in range(1, self.grid.slow + 1):
+            for q in range(1, self.grid.fast):
+                self.push_part(k, q)
 
     def relay(self):
         grid = self.grid
@@ -588,50 +600,254 @@
     )(rows, every_cols, dense_gate, dense_up, gate, up, down)
 
 
-def rms_norm(values, gain):
-    flt = values.astype(jnp.float32)
-    scaled = flt * lax.rsqrt(jnp.mean(flt * flt, axis=-1, keepdims=True) + 1e-06)
-    return (scaled * gain).astype(jnp.bfloat16)
-
-
-def discretize(decay_rate, frequency, log_step, b_real, b_imag):
-    step_size = jnp.exp(log_step)[:, None]
-    lam_re = -decay_rate
+def mixer_kernel(
+    tokens,
+    mix_gain,
+    in_proj_hbm,
+    decay_rate,
+    frequency,
+    log_step,
+    b_real,
+    b_imag,
+    c_real,
+    c_imag,
+    skip_gain,
+    states_hbm,
+    reads,
+    fresh_hbm,
+    in_proj,
+    old,
+    fresh,
+    normed,
+    sems,
+):
+    load_proj = pltpu.make_async_copy(in_proj_hbm, in_proj, sems.at[0])
+    load_old = pltpu.make_async_copy(states_hbm, old, sems.at[1])
+    load_proj.start()
+    load_old.start()
+    count, width = tokens.shape
+    groups, entries = decay_rate.shape
+    channels = skip_gain.shape[1]
+    wide = groups * entries
+    f32, bf16 = jnp.float32, jnp.bfloat16
+
+    def iota(shape, dim):
+        return lax.broadcasted_iota(jnp.int32, shape, dim)
+
+    eye = iota((groups, groups), 0) == iota((groups, groups), 1)
+    step_size = jnp.exp(jnp.sum(jnp.where(eye, log_step[...], 0.0), axis=1, keepdims=True))
+    lam_re, lam_im = -decay_rate[...], frequency[...]
     magnitude = jnp.exp(lam_re * step_size)
-    abar_re = magnitude * jnp.cos(frequency * step_size)
-    abar_im = magnitude * jnp.sin(frequency * step_size)
-    denom = lam_re * lam_re + frequency * frequency
-    fac_re = ((abar_re - 1.0) * lam_re + abar_im * frequency) / denom
-    fac_im = (abar_im * lam_re - (abar_re - 1.0) * frequency) / denom
-    bbar_re = fac_re[..., None] * b_real - fac_im[..., None] * b_imag
-    bbar_im = fac_re[..., None] * b_imag + fac_im[..., None] * b_real
-    return (abar_re, abar_im, bbar_re, bbar_im)
-
-
-def state_step(
-    drive, states, decay_rate, frequency, log_step, b_real, b_imag, c_real, c_imag, skip_gain
+    abar_re = magnitude * jnp.cos(lam_im * step_size)
+    abar_im = magnitude * jnp.sin(lam_im * step_size)
+    denom = lam_re * lam_re + lam_im * lam_im
+    fac_re = ((abar_re - 1.0) * lam_re + abar_im * lam_im) / denom
+    fac_im = (abar_im * lam_re - (abar_re - 1.0) * lam_im) / denom
+    packed = jnp.concatenate([abar_re, abar_im, fac_re, fac_im], axis=0)
+    repeat = (iota((entries, wide), 1) % entries == iota((entries, wide), 0)).astype(f32)
+    spread = jnp.dot(packed, repeat, precision=lax.Precision.HIGHEST, preferred_element_type=f32)
+    owner = iota((groups, wide), 1) // entries == iota((groups, wide), 0)
+
+    def row_of(item):
+        part = spread[item * groups : (item + 1) * groups]
+        return jnp.sum(jnp.where(owner, part, 0.0), axis=0, keepdims=True)
+
+    abar_re, abar_im, fac_re, fac_im = (row_of(item) for item in range(4))
+    inside = iota((wide, channels), 0) // entries == iota((wide, channels), 1) // GROUP
+    place_in = (iota((GROUP, channels), 1) % GROUP == iota((GROUP, channels), 0)).astype(bf16)
+    place_out = (iota((entries, wide), 1) % entries == iota((entries, wide), 0)).astype(bf16)
+    inside_out = iota((channels, wide), 0) // GROUP == iota((channels, wide), 1) // entries
+
+    def in_matrix(ref):
+        flat = ref[...].reshape(wide, GROUP).astype(bf16)
+        full = jnp.dot(flat, place_in, preferred_element_type=f32)
+        return jnp.where(inside, full, 0.0).astype(bf16)
+
+    def out_matrix(ref):
+        flat = ref[...].reshape(channels, entries).astype(bf16)
+        full = jnp.dot(flat, place_out, preferred_element_type=f32)
+        return jnp.where(inside_out, full, 0.0).astype(bf16)
+
+    def by_rows(left, right):
+        return lax.dot_general(
+            left, right, (((1,), (1,)), ((), ())), preferred_element_type=f32
+        )
+
+    step = 16
+    for start in range(0, count, step):
+        flt = tokens[start : start + step, :].astype(f32)
+        scale = lax.rsqrt(jnp.mean(flt * flt, axis=-1, keepdims=True) + 1e-06)
+        normed[start : start + step, :] = (flt * scale * mix_gain[...]).astype(bf16)
+    load_proj.wait()
+    drive = jnp.dot(normed[...], in_proj[...], preferred_element_type=f32).astype(bf16)
+    push_a = by_rows(drive, in_matrix(b_real))
+    push_b = by_rows(drive, in_matrix(b_imag))
+    load_old.wait()
+    old_re, old_im = old[0], old[1]
+    new_re = abar_re * old_re - abar_im * old_im + fac_re * push_a - fac_im * push_b
+    fresh[0] = new_re
+    new_im = abar_re * old_im + abar_im * old_re + fac_re * push_b + fac_im * push_a
+    fresh[1] = new_im
+    store = pltpu.make_async_copy(fresh, fresh_hbm, sems.at[2])
+    store.start()
+    readout = (
+        by_rows(new_re.astype(bf16), out_matrix(c_real))
+        - by_rows(new_im.astype(bf16), out_matrix(c_imag))
+        + skip_gain[...] * drive.astype(f32)
+    )
+    reads[...] = jax.nn.gelu(readout).astype(bf16)
+    store.wait()
+
+
+def mixer(tokens, mix_gain, in_proj, params, skip_gain, states):
+    count = tokens.shape[0]
+    channels = in_proj.shape[1]
+    whole = pl.BlockSpec(memory_space=pltpu.VMEM)
+    far = pl.BlockSpec(memory_space=pl.ANY)
+    return pl.pallas_call(
+        mixer_kernel,
+        out_shape=(
+            jax.ShapeDtypeStruct((count, channels), jnp.bfloat16),
+            jax.ShapeDtypeStruct(states.shape, jnp.float32),
+        ),
+        in_specs=[whole, whole, far] + [whole] * 8 + [far],
+        out_specs=(whole, far),
+        scratch_shapes=[
+            pltpu.VMEM(in_proj.shape, jnp.bfloat16),
+            pltpu.VMEM(states.shape, jnp.float32),
+            pltpu.VMEM(states.shape, jnp.float32),
+            pltpu.VMEM(tokens.shape, jnp.bfloat16),
+            pltpu.SemaphoreType.DMA((3,)),
+        ],
+        compiler_params=pltpu.CompilerParams(vmem_limit_bytes=40 << 20),
+    )(tokens, mix_gain, in_proj, *params, skip_gain, states)
+
+
+def exit_kernel(
+    size,
+    reads,
+    out_proj,
+    tokens,
+    ffn_gain,
+    branch_gate,
+    route_ids,
+    route_logits,
+    own_cols,
+    resid_cols,
+    side,
+    partial,
+    stat,
+    stat_got,
+    stat_sent,
+    stat_landed,
+    *scratch,
 ):
-    count = drive.shape[0]
-    groups = decay_rate.shape[0]
-    abar_re, abar_im, bbar_re, bbar_im = discretize(decay_rate, frequency, log_step, b_real, b_imag)
-    grouped = drive.astype(jnp.float32).reshape(count, groups, GROUP)
-    old_re = states[0].reshape(count, groups, STATE)
-    old_im = states[1].reshape(count, groups, STATE)
-    high = lax.Precision.HIGHEST
-    push_re = jnp.einsum("ngh,gph->ngp", grouped, bbar_re, precision=high)
-    push_im = jnp.einsum("ngh,gph->ngp", grouped, bbar_im, precision=high)
-    new_re = abar_re * old_re - abar_im * old_im + push_re
-    new_im = abar_re * old_im + abar_im * old_re + push_im
-    readout = (
-        jnp.einsum("ngp,ghp->ngh", new_re, c_real, precision=high)
-        - jnp.einsum("ngp,ghp->ngh", new_im, c_imag, precision=high)
-        + skip_gain.reshape(groups, GROUP) * grouped
-    )
-    reads = jax.nn.gelu(readout.reshape(count, groups * GROUP)).astype(jnp.bfloat16)
-    fresh = jnp.stack(
-        [new_re.reshape(count, groups * STATE), new_im.reshape(count, groups * STATE)]
-    )
-    return (reads, fresh)
+    f32, bf16 = jnp.float32, jnp.bfloat16
+    grid = Grid("tp", size)
+    mix = Reduce(grid, partial, MIX_PIECES, True, scratch)
+    count, width = resid_cols.shape
+    grid.greet_all()
+
+    def block(dest):
+        span = pl.ds(pl.multiple_of(dest * width, 128), width)
+        partial[:, span] = jnp.dot(
+            reads[...], out_proj[:, span], preferred_element_type=f32
+        ).astype(bf16)
+
+    for k in range(1, grid.slow + 1):
+        for q in range(1, grid.fast):
+            block(grid.index(k, q))
+            mix.push_part(k, q)
+    for k in range(1, grid.slow + 1):
+        block(grid.index(k, 0))
+    logits = route_logits[...]
+    top = logits.shape[1]
+    raised = jnp.exp(logits - jnp.max(logits, axis=1, keepdims=True))
+    weights = raised / jnp.sum(raised, axis=1, keepdims=True)
+    ids = route_ids[...].astype(f32)
+    mix.relay()
+    mine = pl.ds(pl.multiple_of(grid.me * width, 128), width)
+    gain = ffn_gain[:, mine]
+    gate = gain * branch_gate[:, mine]
+    lanes = lax.broadcasted_iota(jnp.int32, (count, 128), 1)
+    ssq_parts, dot_parts = [], []
+
+    def emit(span, value):
+        mixed = value.astype(bf16).astype(f32)
+        resid = (tokens[span, mine].astype(f32) + mixed).astype(bf16)
+        resid_cols[span, :] = resid
+        flt = resid.astype(f32)
+        ssq_parts.append(jnp.sum(flt * flt, axis=1, keepdims=True))
+        dot_parts.append(jnp.sum(flt * gate, axis=1, keepdims=True))
+
+    mix.collect(emit)
+    ssq, dots = jnp.concatenate(ssq_parts, axis=0), jnp.concatenate(dot_parts, axis=0)
+    table = jnp.where(lanes == 0, ssq, jnp.where(lanes == 1, dots, 0.0))
+    for item in range(top):
+        table = jnp.where(lanes == 2 + item, ids[:, item : item + 1], table)
+        table = jnp.where(lanes == 2 + top + item, weights[:, item : item + 1], table)
+    if count < 128:
+        table = jnp.concatenate([table, jnp.zeros((128 - count, 128), f32)], axis=0)
+    turned = table.T
+    stat[...] = turned[:8]
+    copies = []
+    for k in range(1, size):
+        copy = grid.copy(
+            stat,
+            stat_got.at[k - 1],
+            stat_sent.at[k - 1],
+            stat_landed.at[k - 1],
+            (grid.me + k) % size,
+        )
+        copy.start()
+        copies.append(copy)
+    total = turned[:8]
+    for copy in copies:
+        copy.wait_recv()
+    for k in range(1, size):
+        total = total + stat_got[k - 1]
+    scale = lax.rsqrt(total[0:1] / (width * size) + 1e-06)
+    branch = jax.nn.sigmoid(total[1:2] * scale)
+    rows = lax.broadcasted_iota(jnp.int32, (8, 128), 0)
+    shifted = jnp.concatenate([turned[2 : 2 + 2 * top], jnp.zeros((8 - 2 * top, 128), f32)], axis=0)
+    side[...] = jnp.where(rows == 2 * top, branch, shifted)
+    column = jnp.broadcast_to(scale, (128, 128)).T[:count, 0:1]
+    own_cols[...] = (resid_cols[...].astype(f32) * column * gain).astype(bf16)
+    for copy in copies:
+        copy.wait_send()
+    mix.finish()
+
+
+MIX_PIECES = 2
+
+
+def mixer_exit(reads, out_proj, tokens, ffn_gain, branch_gate, route_ids, route_logits, size):
+    count, width = tokens.shape
+    part = width // size
+    fast = fast_extent("tp", size)
+    bf16 = jnp.bfloat16
+    whole = pl.BlockSpec(memory_space=pltpu.VMEM)
+    return pl.pallas_call(
+        functools.partial(exit_kernel, size),
+        out_shape=(
+            jax.ShapeDtypeStruct((count, part), bf16),
+            jax.ShapeDtypeStruct((count, part), bf16),
+            jax.ShapeDtypeStruct((8, 128), jnp.float32),
+        ),
+        in_specs=[whole] * 7,
+        out_specs=(whole,) * 3,
+        scratch_shapes=[
+            pltpu.VMEM((count, width), bf16),
+            pltpu.VMEM((8, 128), jnp.float32),
+            pltpu.VMEM((size - 1, 8, 128), jnp.float32),
+            pltpu.SemaphoreType.DMA((size - 1,)),
+            pltpu.SemaphoreType.DMA((size - 1,)),
+        ]
+        + reduce_scratch(fast, size // fast, count, part, MIX_PIECES),
+        compiler_params=pltpu.CompilerParams(
+            collective_id=0, has_side_effects=True, vmem_limit_bytes=24 << 20
+        ),
+    )(reads, out_proj, tokens, ffn_gain, branch_gate, route_ids, route_logits)
 
 
 def shards(
@@ -662,30 +878,30 @@
     seq_count, width = tokens.shape
     tp_count = lax.axis_size("tp")
     ep_count = lax.axis_size("ep")
-    tp_index = lax.axis_index("tp")
     part_width = width // tp_count
-    normed = rms_norm(tokens, mix_gain)
-    drive = jnp.dot(normed, in_proj, preferred_element_type=jnp.float32).astype(jnp.bfloat16)
-    reads, new_states = state_step(
-        drive, states, decay_rate, frequency, log_step, b_real, b_imag, c_real, c_imag, skip_gain
+    params = (
+        decay_rate,
+        frequency,
+        log_step.reshape(1, -1),
+        b_real,
+        b_imag,
+        c_real,
+        c_imag,
     )
-    partial_value = (
-        jnp.dot(reads, out_proj, preferred_element_type=jnp.float32)
-        .astype(jnp.bfloat16)
-        .astype(jnp.float32)
+    reads, new_states = mixer(
+        tokens, mix_gain.reshape(1, -1), in_proj, params, skip_gain.reshape(1, -1), states
     )
-    mixed_cols = reduce_scatter(partial_value.astype(jnp.bfloat16), "tp", tp_count, 2, True, 0)
-    (mixed,) = all_gather([mixed_cols], "tp", tp_count, [2], True, 1)
-    resid = (tokens.astype(jnp.float32) + mixed.astype(jnp.float32)).astype(jnp.bfloat16)
-    normed_two = rms_norm(resid, ffn_gain)
-    own_cols = lax.dynamic_slice_in_dim(normed_two, tp_index * part_width, part_width, 1)
-    branch = jax.nn.sigmoid(jnp.dot(normed_two, branch_gate, preferred_element_type=jnp.float32))
-    route_weights = jax.nn.softmax(route_logits, axis=-1)
+    own_cols, resid_cols, side = mixer_exit(
+        reads,
+        out_proj,
+        tokens,
+        ffn_gain.reshape(1, -1),
+        branch_gate.astype(jnp.float32).reshape(1, -1),
+        route_ids,
+        route_logits,
+        tp_count,
+    )
     top_count = route_ids.shape[1]
-    side = jnp.concatenate(
-        [route_ids.astype(jnp.float32).T, route_weights.T, branch[None, :]], axis=0
-    )
-    side = jnp.pad(side, ((0, -side.shape[0] % 8), (0, -seq_count % 128)))
     every_cols, every_side = all_gather([own_cols, side], "ep", ep_count, [2, 1], False, 2)
     total_count = ep_count * seq_count
     every_cols = every_cols.reshape(total_count, part_width)
@@ -724,7 +940,6 @@
     share = (routed_part + every_branch[:, None] * dense_part).astype(jnp.bfloat16)
     share = share.reshape(ep_count, seq_count, part_width)
     gathered = reduce_scatter(share, "ep", ep_count, 2, False, 4)
-    resid_cols = lax.dynamic_slice_in_dim(resid, tp_index * part_width, part_width, 1)
     output = (resid_cols.astype(jnp.float32) + gathered.astype(jnp.float32)).astype(jnp.bfloat16)
     return (output, new_states)
 

time: 165 us -> 152 us (0.921)
  matrix products: 15.1 us -> 5.39 us
  other arithmetic: 10 us -> 2.33 us
  local copies, waits for them, and re-layouts: 6.79 us -> 12.3 us
    pallas_call x0 -> x2, Pallas kernels: none -> 17.8 us  [the longest x1 13.9 us: mixer_exit(): pl.pallas_call(functools.partial(exit_kernel, size), out_shape=(jax.Shape...]
    pallas_call x2 -> x1, Pallas kernels: 35.1 us -> 24.7 us  [reduce_scatter(): pl.pallas_call(functools.partial(reduce_kernel, axis, size, number, cols)...]
    unnamed x31 -> x34, local copies, waits for them, and re-layouts: 1.96 us -> 11.8 us
    pallas_call x2 -> x1, Pallas kernels: 35.9 us -> 27.3 us  [all_gather(): pl.pallas_call(functools.partial(gather_kernel, axis, size, pieces, cols)...]
    dot_general x7 -> x0, matrix products: 8.19 us -> none  [the longest x1 2.37 us: shards(): jnp.dot(normed, in_proj, preferred_element_type=jnp.float32)]
    transpose x2 -> x0, other arithmetic: 2.52 us -> none  [the longest x1 1.29 us: shards(): side = jnp.concatenate([route_ids.astype(jnp.float32).T, route_weights.T,...]
    reduce_sum x3 -> x0, other arithmetic: 2.46 us -> none  [the longest x2 1.76 us: rms_norm(): jnp.mean(flt * flt, axis=-1, keepdims=True) + 1e-06]
    slice x4 -> x1, local copies, waits for them, and re-layouts: 2.44 us -> 0.07 us  [the longest x2 1.37 us: state_step(): old_re = states[0].reshape(count, groups, STATE)]
where the time goes in v1:
time: 152 us
  Pallas kernels  131 us (86%)
  local copies, waits for them, and re-layouts  12.3 us (8%)
  matrix products  5.39 us (4%)
  other arithmetic  2.33 us (2%)
    pallas_call x1, Pallas kernels, branches(): pl.pallas_call(functools.partial(branches_kernel, axis, size), out_shape=...  61.1 us
    pallas_call x1, Pallas kernels, all_gather(): pl.pallas_call(functools.partial(gather_kernel, axis, size, pieces, cols)...  27.3 us
    pallas_call x1, Pallas kernels, reduce_scatter(): pl.pallas_call(functools.partial(reduce_kernel, axis, size, number, cols)...  24.7 us
    pallas_call x1, Pallas kernels, mixer_exit(): pl.pallas_call(functools.partial(exit_kernel, size), out_shape=(jax.Shape...  13.9 us
    unnamed x34, local copies, waits for them, and re-layouts  11.8 us
    pallas_call x1, Pallas kernels, mixer(): pl.pallas_call(mixer_kernel, out_shape=(jax.ShapeDtypeStruct((count, chan...  3.87 us

profile of v1, /device:TPU:0, one launch (start us, length us, event | category | flops | bytes accessed | tf_op | source)
XLA Modules:
  0.0 151.8 jit_solution(16178671660361882264)
XLA Ops:
  0.6 0.0 copy-start
  0.6 0.0 copy-start.1
  0.7 0.9 reshape.83
  1.5 0.8 copy.35.route_ids
  2.3 0.8 copy.36.route_logits
  3.1 1.1 copy.33.b_real
  4.2 1.1 copy.34.b_imag
  5.3 0.0 copy-done.1
  5.3 0.0 copy-start.3
  5.3 1.6 %copy-done.3 = bf16[4096,256]{1,0:T(8,128)(2,1)S(1)} copy-done((bf16[4096,256]{1,0:T(8,128)(2,1)S(1)}, bf16[4096,256]{1,0:T(8,128)(2,1)}, u32[]{:S(2)}) %copy-start.3) | copy-done | bytes 2097176
  6.9 0.0 copy-start.5
  6.9 1.1 copy-done.5
  8.0 0.0 copy-start.6
  8.0 0.9 copy-done.6
  8.9 0.0 copy-start.7
  8.9 0.9 copy-done.7
  9.8 0.0 copy-start.8
  9.8 0.7 copy-done.8
  10.6 0.0 copy-start.10
  10.6 0.7 copy-done.10
  11.3 0.0 copy-start.11
  11.3 0.7 copy-done.11
  12.0 0.0 copy-start.12
  12.0 0.7 copy-done.12
  12.6 0.0 copy-start.13
  12.6 0.7 copy-done.13
  13.3 0.0 copy-start.2
  13.3 0.0 copy-start.9
  13.3 3.9 %shard_map.230 = (bf16[96,256]{1,0:T(8,128)(2,1)S(1)}, f32[2,96,1024]{2,1,0:T(8,128)}) custom-call(bf16[96,4096]{1,0:T(8,128)(2,1)S(1)} %copy-done.1, f32[1,4096]{1,0:T(1,128)S(1)} %bitcast.22, bf16[4096,256]{1,0:T(8,128)(2,1)S(1)} %copy-done.3, f32[16,64]{1,0:T(8,128)S(1)} %copy-done.10, f32[16,64]{1,0:T(8,128)S(1)} %copy-done.11, f32[1,16]{1,0:T(1,128)S(1)} %bitcast.25, ...), custom_call_target="tpu_custom_call" | custom-call | tf_op jit(solution)/shard_map/pallas_call | solution.py:707
  17.2 0.0 copy-done.2
  17.2 0.0 copy-done.9
  17.2 13.9 %shard_map.231 = (bf16[96,1024]{1,0:T(8,128)(2,1)S(1)}, bf16[96,1024]{1,0:T(8,128)(2,1)S(1)}, f32[8,128]{1,0:T(8,128)S(1)}) custom-call(bf16[96,256]{1,0:T(8,128)(2,1)S(1)} %get-tuple-element.11.reads, bf16[256,4096]{1,0:T(8,128)(2,1)S(1)} %copy-done.2, bf16[96,4096]{1,0:T(8,128)(2,1)S(1)} %copy-done.1, f32[1,4096]{1,0:T(1,128)S(1)} %bitcast.23, ...), custom_call_target="tpu_custom_call" | custom-call | tf_op jit(solution)/shard_map/pallas_call | solution.py:830
  31.1 27.3 %shard_map.232 = (bf16[8,96,1024]{2,1,0:T(8,128)(2,1)S(1)}, f32[8,8,128]{2,1,0:T(8,128)S(1)}) custom-call(bf16[96,1024]{1,0:T(8,128)(2,1)S(1)} %get-tuple-element.13.refs_0_, f32[8,128]{1,0:T(8,128)S(1)} %get-tuple-element.14.refs_1_), custom_call_target="tpu_custom_call" | custom-call | tf_op jit(solution)/shard_map/pallas_call | solution.py:174
  58.4 0.0 copy-start.4
  58.4 0.1 reduce_or.12
  58.5 0.1 reshape.85
  58.6 0.3 reduce-window.9
  58.9 0.1 mul.20
  59.0 0.1 reduce_sum.21
  59.1 0.1 slice.24
  59.2 0.1 slice_reduce_fusion.1
  59.3 0.1 add_bitcast_fusion
  59.4 0.3 select_reduce_fusion
  59.7 1.7 %convolution_convert_fusion.rows_ref = bf16[384,1024]{1,0:T(8,128)(2,1)} fusion(bf16[768,1024]{1,0:T(8,128)(2,1)S(1)} %bitcast.18, s32[768]{0:T(1024)S(1)} %add_bitcast_fusion, pred[768]{0:T(1024)(128)(4,1)S(1)} %reduce_or.12), kind=kOutput, calls=%fused_computation.2 | convolution fusion | flops 604962816 | bytes 2363136 | tf_op jit(solution)/shard_map/dot_general | solution.py:921
  61.4 0.0 copy-done.4
  61.4 61.1 %shard_map.233 = (bf16[4,192,768]{2,1,0:T(8,128)(2,1)}, bf16[384,1024]{1,0:T(8,128)(2,1)}) custom-call(bf16[384,1024]{1,0:T(8,128)(2,1)} %convolution_convert_fusion.rows_ref, bf16[768,1024]{1,0:T(8,128)(2,1)} %bitcast.19, bf16[1024,768]{1,0:T(8,128)(2,1)} %dense_gate.1, bf16[1024,768]{1,0:T(8,128)(2,1)} %dense_up.1, bf16[4096,768]{1,0:T(8,128)(2,1)} %bitcast.26, ...), custom_call_target="tpu_custom_call" | custom-call | tf_op jit(solution)/shard_map/pallas_call | solution.py:574
  122.5 0.0 copy-start.14
  122.5 2.3 %fusion.1 = f32[768,1024]{1,0:T(8,128)S(1)} fusion(bf16[384,1024]{1,0:T(8,128)(2,1)} %get-tuple-element.17, f32[384]{0:T(512)S(1)} %select_reduce_fusion, s32[768]{0:T(1024)S(1)} %add_bitcast_fusion, pred[768]{0:T(1024)(128)(4,1)S(1)} %reduce_or.12), kind=kOutput, calls=%fused_computation.6 | convolution fusion | flops 605749248 | bytes 3937536 | tf_op jit(solution)/shard_map/dot_general | solution.py:936
  124.9 0.0 copy-done
  124.9 0.0 copy-done.14
  124.9 1.4 add_convert_fusion
  126.3 24.7 %shard_map.234 = bf16[96,1024]{1,0:T(8,128)(2,1)S(1)} custom-call(bf16[8,96,1024]{2,1,0:T(8,128)(2,1)S(1)} %bitcast.20), custom_call_target="tpu_custom_call" | custom-call | tf_op jit(solution)/shard_map/pallas_call | solution.py:273
  151.0 0.7 add_convert_fusion.1
  (6 shorter events, 0.1 us)
Async XLA Ops:
  0.6 124.3 %copy-start = (bf16[768,1024]{1,0:T(8,128)(2,1)S(1)}, bf16[768,1024]{1,0:T(8,128)(2,1)}, u32[]{:S(2)}) copy-start(bf16[768,1024]{1,0:T(8,128)(2,1)} %param.44) | copy-start | bytes 4718596
  0.6 4.6 %copy-start.1 = (bf16[96,4096]{1,0:T(8,128)(2,1)S(1)}, bf16[96,4096]{1,0:T(8,128)(2,1)}, u32[]{:S(2)}) copy-start(bf16[96,4096]{1,0:T(8,128)(2,1)} %tokens.3) | copy-start | bytes 2359300
  5.3 1.6 %copy-start.3 = (bf16[4096,256]{1,0:T(8,128)(2,1)S(1)}, bf16[4096,256]{1,0:T(8,128)(2,1)}, u32[]{:S(2)}) copy-start(bf16[4096,256]{1,0:T(8,128)(2,1)} %in_proj_hbm.1) | copy-start | bytes 6291460
  6.9 1.1 copy-start.5
  8.0 0.9 copy-start.6
  8.9 0.9 copy-start.7
  9.8 0.7 copy-start.8
  10.6 0.7 copy-start.10
  11.3 0.7 copy-start.11
  12.0 0.7 copy-start.12
  12.6 0.7 copy-start.13
  13.3 3.9 %copy-start.2 = (bf16[256,4096]{1,0:T(8,128)(2,1)S(1)}, bf16[256,4096]{1,0:T(8,128)(2,1)}, u32[]{:S(2)}) copy-start(bf16[256,4096]{1,0:T(8,128)(2,1)} %out_proj.1) | copy-start | bytes 6291460
  13.3 3.9 %copy-start.9 = (f32[4096]{0:T(1024)S(1)}, f32[4096]{0:T(1024)}, u32[]{:S(2)}) copy-start(f32[4096]{0:T(1024)} %param.25) | copy-start | bytes 49156
  58.4 3.0 %copy-start.4 = (bf16[8,96,1024]{2,1,0:T(8,128)(2,1)}, bf16[8,96,1024]{2,1,0:T(8,128)(2,1)S(1)}, u32[]{:S(2)}) copy-start(bf16[8,96,1024]{2,1,0:T(8,128)(2,1)S(1)} %get-tuple-element.16) | copy-start | bytes 4718596
  122.5 2.4 %copy-start.14 = (bf16[4,192,768]{2,1,0:T(8,128)(2,1)S(1)}, bf16[4,192,768]{2,1,0:T(8,128)(2,1)}, u32[]{:S(2)}) copy-start(bf16[4,192,768]{2,1,0:T(8,128)(2,1)} %get-tuple-element.18) | copy-start | bytes 3538948

commit v2 on v1

v2 whole, which is shorter than its diff:
```python
import functools
import jax
import jax.numpy as jnp
from jax import lax
from jax.experimental import pallas as pl
from jax.experimental.pallas import tpu as pltpu
from jax.sharding import PartitionSpec as P

GROUP = 16
STATE = 64
MESH = pl.DeviceIdType.MESH


def fast_extent(axis, size):
    if axis == "tp":
        return 2
    extent = 1
    while (2 * extent) * (2 * extent) * 2 <= size:
        extent *= 2
    return extent


class Grid:
    def __init__(self, axis, size):
        self.axis, self.size = axis, size
        self.fast = fast_extent(axis, size)
        self.slow = size // self.fast
        self.me = lax.axis_index(axis)
        self.at_fast = self.me % self.fast
        self.at_slow = self.me // self.fast

    def index(self, slow_step, fast_step):
        slow_at = (self.at_slow + slow_step + self.slow) % self.slow
        fast_at = (self.at_fast + fast_step + self.fast) % self.fast
        return slow_at * self.fast + fast_at

    def peers(self):
        return [self.index(k, 0) for k in range(1, self.slow)] + [
            self.index(0, q) for q in range(1, self.fast)
        ]

    def greet(self):
        barrier = pltpu.get_barrier_semaphore()
        peers = self.peers()
        for peer in peers:
            pl.semaphore_signal(barrier, inc=1, device_id={self.axis: peer}, device_id_type=MESH)
        pl.semaphore_wait(barrier, len(peers))

    def greet_all(self):
        barrier = pltpu.get_barrier_semaphore()
        for k in range(1, self.size):
            pl.semaphore_signal(
                barrier,
                inc=1,
                device_id={self.axis: (self.me + k) % self.size},
                device_id_type=MESH,
            )
        pl.semaphore_wait(barrier, self.size - 1)

    def copy(self, source, target, sent, landed, peer):
        return pltpu.make_async_remote_copy(
            src_ref=source,
            dst_ref=target,
            send_sem=sent,
            recv_sem=landed,
            device_id={self.axis: peer},
            device_id_type=MESH,
        )


def part_of(ref, owner, start, rows, width, cols):
    if cols:
        return ref.at[pl.ds(start, rows), pl.ds(pl.multiple_of(owner * width, 128), width)]
    return ref.at[owner, pl.ds(start, rows), :]


class Gather:
    def __init__(self, grid, source, target, number, cols, sems, shape=None):
        self.grid, self.source, self.target, self.cols = grid, source, target, cols
        self.slow_sent, self.slow_landed, self.fast_sent, self.fast_landed, self.own_sem = sems
        self.rows, self.width = shape or source.shape
        self.step = self.rows // number
        self.number = number
        self.pending = []

    def piece(self, j):
        if self.source is None:
            return self.place(self.grid.me, j)
        return self.source.at[pl.ds(j * self.step, self.step), :]

    def place(self, owner, j):
        return part_of(self.target, owner, j * self.step, self.step, self.width, self.cols)

    def slow_copy(self, source, target, j, k, peer):
        return self.grid.copy(
            source, target, self.slow_sent.at[j, k - 1], self.slow_landed.at[j, k - 1], peer
        )

    def fast_copy(self, source, target, j, k, q, peer):
        return self.grid.copy(
            source, target, self.fast_sent.at[j, k, q - 1], self.fast_landed.at[j, k, q - 1], peer
        )

    def launch(self, copy):
        copy.start()
        self.pending.append(copy)

    def start_piece(self, j):
        grid = self.grid
        piece, spot = self.piece(j), self.place(grid.me, j)
        for k in range(1, grid.slow):
            self.launch(self.slow_copy(piece, spot, j, k, grid.index(k, 0)))
        for q in range(1, grid.fast):
            self.launch(self.fast_copy(piece, spot, j, 0, q, grid.index(0, q)))

    def start(self):
        for j in range(self.number):
            self.start_piece(j)
        if self.source is not None:
            self.own = pltpu.make_async_copy(
                self.source,
                part_of(self.target, self.grid.me, 0, self.rows, self.width, self.cols),
                self.own_sem,
            )
            self.own.start()

    def relay(self):
        grid = self.grid
        for j in range(self.number):
            for k in range(1, grid.slow):
                spot = self.place(grid.index(-k, 0), j)
                self.slow_copy(spot, spot, j, k, grid.index(-k, 0)).wait_recv()
                for q in range(1, grid.fast):
                    self.launch(self.fast_copy(spot, spot, j, k, q, grid.index(0, q)))

    def arrive(self):
        grid = self.grid
        for j in range(self.number):
            for k in range(grid.slow):
                for q in range(1, grid.fast):
                    spot = self.place(grid.index(-k, -q), j)
                    self.fast_copy(spot, spot, j, k, q, grid.index(0, -q)).wait_recv()
        if self.source is not None:
            self.own.wait()

    def finish(self):
        for copy in self.pending:
            copy.wait_send()


def gather_sems(grid_fast, grid_slow, number):
    return [
        pltpu.SemaphoreType.DMA((number, grid_slow - 1)),
        pltpu.SemaphoreType.DMA((number, grid_slow - 1)),
        pltpu.SemaphoreType.DMA((number, grid_slow, grid_fast - 1)),
        pltpu.SemaphoreType.DMA((number, grid_slow, grid_fast - 1)),
        pltpu.SemaphoreType.DMA,
    ]


class Reduce:
    def __init__(self, grid, source, number, cols, scratch):
        self.grid, self.source, self.cols, self.number = grid, source, cols, number
        self.got_fast, self.mid, self.got_slow, self.total = scratch[:4]
        self.fast_sent, self.fast_landed, self.slow_sent, self.slow_landed = scratch[4:]
        rows, self.width = self.total.shape
        self.step = rows // number
        self.pending = []

    def part(self, dest, j):
        return part_of(self.source, dest, j * self.step, self.step, self.width, self.cols)

    def span(self, j):
        return pl.ds(j * self.step, self.step)

    def fast_copy(self, source, k, j, q, peer):
        return self.grid.copy(
            source,
            self.got_fast.at[q - 1, k - 1, self.span(j), :],
            self.fast_sent.at[q - 1, k - 1, j],
            self.fast_landed.at[q - 1, k - 1, j],
            peer,
        )

    def slow_copy(self, k, j, peer):
        return self.grid.copy(
            self.mid.at[k - 1, self.span(j), :],
            self.got_slow.at[k - 1, self.span(j), :],
            self.slow_sent.at[k - 1, j],
            self.slow_landed.at[k - 1, j],
            peer,
        )

    def push_part(self, k, q):
        grid = self.grid
        for j in range(self.number):
            copy = self.fast_copy(self.part(grid.index(k, q), j), k, j, q, grid.index(0, q))
            copy.start()
            self.pending.append(copy)

    def push(self):
        for k in range(1, self.grid.slow + 1):
            for q in range(1, self.grid.fast):
                self.push_part(k, q)

    def relay(self):
        grid = self.grid
        for k in range(1, grid.slow + 1):
            for j in range(self.number):
                value = self.part(grid.index(k, 0), j)[...].astype(jnp.float32)
                for q in range(1, grid.fast):
                    block = self.got_fast.at[q - 1, k - 1, self.span(j), :]
                    self.fast_copy(block, k, j, q, grid.index(0, -q)).wait_recv()
                    value = value + block[...].astype(jnp.float32)
                if k == grid.slow:
                    self.total[self.span(j), :] = value
                else:
                    self.mid[k - 1, self.span(j), :] = value.astype(self.mid.dtype)
                    copy = self.slow_copy(k, j, grid.index(k, 0))
                    copy.start()
                    self.pending.append(copy)

    def collect_piece(self, j):
        value = self.total[self.span(j), :]
        for k in range(1, self.grid.slow):
            self.slow_copy(k, j, self.grid.index(-k, 0)).wait_recv()
            value = value + self.got_slow[k - 1, self.span(j), :].astype(jnp.float32)
        return value

    def collect(self, emit):
        for j in range(self.number):
            emit(self.span(j), self.collect_piece(j))

    def finish(self):
        for copy in self.pending:
            copy.wait_send()


def reduce_scratch(fast, slow, rows, width, number):
    return [
        pltpu.VMEM((fast - 1, slow, rows, width), jnp.bfloat16),
        pltpu.VMEM((slow - 1, rows, width), jnp.bfloat16),
        pltpu.VMEM((slow - 1, rows, width), jnp.bfloat16),
        pltpu.VMEM((rows, width), jnp.float32),
        pltpu.SemaphoreType.DMA((fast - 1, slow, number)),
        pltpu.SemaphoreType.DMA((fast - 1, slow, number)),
        pltpu.SemaphoreType.DMA((slow - 1, number)),
        pltpu.SemaphoreType.DMA((slow - 1, number)),
    ]


def tile_of(extent):
    for tile in (256, 128):
        if extent % tile == 0:
            return tile
    return extent


def mixer_kernel(
    *refs,
):
    far, reads, fresh_hbm = refs[:12], refs[12], refs[13]
    near, fresh, normed, sems = refs[14:26], refs[26], refs[27], refs[28]
    loads = []
    for item, (source, target) in enumerate(zip(far, near)):
        load = pltpu.make_async_copy(source, target, sems.at[item])
        load.start()
        loads.append(load)
    tokens, mix_gain, in_proj, decay_rate, frequency, log_step = near[:6]
    b_real, b_imag, c_real, c_imag, skip_gain, old = near[6:]
    count, width = tokens.shape
    groups, entries = decay_rate.shape
    channels = skip_gain.shape[1]
    wide = groups * entries
    f32, bf16 = jnp.float32, jnp.bfloat16

    def iota(shape, dim):
        return lax.broadcasted_iota(jnp.int32, shape, dim)

    for item in range(3, 6):
        loads[item].wait()
    eye = iota((groups, groups), 0) == iota((groups, groups), 1)
    step_size = jnp.exp(jnp.sum(jnp.where(eye, log_step[...], 0.0), axis=1, keepdims=True))
    lam_re, lam_im = -decay_rate[...], frequency[...]
    magnitude = jnp.exp(lam_re * step_size)
    abar_re = magnitude * jnp.cos(lam_im * step_size)
    abar_im = magnitude * jnp.sin(lam_im * step_size)
    denom = lam_re * lam_re + lam_im * lam_im
    fac_re = ((abar_re - 1.0) * lam_re + abar_im * lam_im) / denom
    fac_im = (abar_im * lam_re - (abar_re - 1.0) * lam_im) / denom
    packed = jnp.concatenate([abar_re, abar_im, fac_re, fac_im], axis=0)
    repeat = (iota((entries, wide), 1) % entries == iota((entries, wide), 0)).astype(f32)
    spread = jnp.dot(packed, repeat, precision=lax.Precision.HIGHEST, preferred_element_type=f32)
    owner = iota((groups, wide), 1) // entries == iota((groups, wide), 0)

    def row_of(item):
        part = spread[item * groups : (item + 1) * groups]
        return jnp.sum(jnp.where(owner, part, 0.0), axis=0, keepdims=True)

    abar_re, abar_im, fac_re, fac_im = (row_of(item) for item in range(4))
    repeat = repeat.astype(bf16)
    inside = iota((channels, wide), 0) // GROUP == iota((channels, wide), 1) // entries

    def matrix(ref):
        flat = ref[...].reshape(channels, entries).astype(bf16)
        full = jnp.dot(flat, repeat, preferred_element_type=f32)
        return jnp.where(inside, full, 0.0).astype(bf16)

    def by_rows(left, right):
        return lax.dot_general(
            left, right, (((1,), (1,)), ((), ())), preferred_element_type=f32
        )

    loads[0].wait()
    loads[1].wait()
    step = 16
    for start in range(0, count, step):
        flt = tokens[start : start + step, :].astype(f32)
        scale = lax.rsqrt(jnp.mean(flt * flt, axis=-1, keepdims=True) + 1e-06)
        normed[start : start + step, :] = (flt * scale * mix_gain[...]).astype(bf16)
    loads[2].wait()
    drive = jnp.dot(normed[...], in_proj[...], preferred_element_type=f32).astype(bf16)
    for load in loads[6:]:
        load.wait()
    push_a = jnp.dot(drive, matrix(b_real), preferred_element_type=f32)
    push_b = jnp.dot(drive, matrix(b_imag), preferred_element_type=f32)
    old_re, old_im = old[0], old[1]
    new_re = abar_re * old_re - abar_im * old_im + fac_re * push_a - fac_im * push_b
    fresh[0] = new_re
    new_im = abar_re * old_im + abar_im * old_re + fac_re * push_b + fac_im * push_a
    fresh[1] = new_im
    store = pltpu.make_async_copy(fresh, fresh_hbm, sems.at[12])
    store.start()
    readout = (
        by_rows(new_re.astype(bf16), matrix(c_real))
        - by_rows(new_im.astype(bf16), matrix(c_imag))
        + skip_gain[...] * drive.astype(f32)
    )
    reads[...] = jax.nn.gelu(readout).astype(bf16)
    store.wait()


def mixer(*arrays):
    tokens, in_proj, states = arrays[0], arrays[2], arrays[-1]
    far = pl.BlockSpec(memory_space=pl.ANY)
    return pl.pallas_call(
        mixer_kernel,
        out_shape=(
            jax.ShapeDtypeStruct((tokens.shape[0], in_proj.shape[1]), jnp.bfloat16),
            jax.ShapeDtypeStruct(states.shape, jnp.float32),
        ),
        in_specs=[far] * len(arrays),
        out_specs=(pl.BlockSpec(memory_space=pltpu.VMEM), far),
        scratch_shapes=[pltpu.VMEM(array.shape, array.dtype) for array in arrays]
        + [
            pltpu.VMEM(states.shape, jnp.float32),
            pltpu.VMEM(tokens.shape, jnp.bfloat16),
            pltpu.SemaphoreType.DMA((13,)),
        ],
        compiler_params=pltpu.CompilerParams(vmem_limit_bytes=62 << 20),
    )(*arrays)


def exit_kernel(
    size,
    reads,
    out_proj_hbm,
    tokens_hbm,
    ffn_gain,
    branch_gate,
    route_ids,
    route_logits,
    own_cols,
    resid_cols,
    side,
    out_proj,
    tokens,
    load_sems,
    partial,
    stat,
    stat_got,
    stat_sent,
    stat_landed,
    *scratch,
):
    f32, bf16 = jnp.float32, jnp.bfloat16
    grid = Grid("tp", size)
    mix = Reduce(grid, partial, MIX_PIECES, True, scratch)
    count, width = resid_cols.shape
    mine = pl.ds(pl.multiple_of(grid.me * width, 128), width)
    loads = [
        pltpu.make_async_copy(out_proj_hbm, out_proj, load_sems.at[0]),
        pltpu.make_async_copy(tokens_hbm.at[:, mine], tokens, load_sems.at[1]),
    ]
    for load in loads:
        load.start()
    grid.greet_all()
    for load in loads:
        load.wait()

    def block(dest):
        span = pl.ds(pl.multiple_of(dest * width, 128), width)
        partial[:, span] = jnp.dot(
            reads[...], out_proj[:, span], preferred_element_type=f32
        ).astype(bf16)

    for k in range(1, grid.slow + 1):
        for q in range(1, grid.fast):
            block(grid.index(k, q))
            mix.push_part(k, q)
    for k in range(1, grid.slow + 1):
        block(grid.index(k, 0))
    logits = route_logits[...]
    top = logits.shape[0]
    raised = jnp.exp(logits - jnp.max(logits, axis=0, keepdims=True))
    weights = raised / jnp.sum(raised, axis=0, keepdims=True)
    side[...] = jnp.zeros((8, 128), f32)
    side[0:top, 0:count] = route_ids[...].astype(f32)
    side[top : 2 * top, 0:count] = weights
    mix.relay()
    gain = ffn_gain[:, mine]
    gate = gain * branch_gate[:, mine]
    lanes = lax.broadcasted_iota(jnp.int32, (count, 128), 1)
    ssq_parts, dot_parts = [], []

    def emit(span, value):
        mixed = value.astype(bf16).astype(f32)
        resid = (tokens[span, :].astype(f32) + mixed).astype(bf16)
        resid_cols[span, :] = resid
        flt = resid.astype(f32)
        ssq_parts.append(jnp.sum(flt * flt, axis=1, keepdims=True))
        dot_parts.append(jnp.sum(flt * gate, axis=1, keepdims=True))

    mix.collect(emit)
    ssq, dots = jnp.concatenate(ssq_parts, axis=0), jnp.concatenate(dot_parts, axis=0)
    table = jnp.where(lanes == 0, ssq, jnp.where(lanes == 1, dots, 0.0))
    if count < 128:
        table = jnp.concatenate([table, jnp.zeros((128 - count, 128), f32)], axis=0)
    turned = table.T
    stat[...] = turned[:8]
    copies = []
    for k in range(1, size):
        copy = grid.copy(
            stat,
            stat_got.at[k - 1],
            stat_sent.at[k - 1],
            stat_landed.at[k - 1],
            (grid.me + k) % size,
        )
        copy.start()
        copies.append(copy)
    total = turned[:8]
    for copy in copies:
        copy.wait_recv()
    for k in range(1, size):
        total = total + stat_got[k - 1]
    scale = lax.rsqrt(total[0:1] / (width * size) + 1e-06)
    branch = jax.nn.sigmoid(total[1:2] * scale)
    side[2 * top : 2 * top + 1, :] = branch
    column = jnp.broadcast_to(scale, (128, 128)).T[:count, 0:1]
    own_cols[...] = (resid_cols[...].astype(f32) * column * gain).astype(bf16)
    for copy in copies:
        copy.wait_send()
    mix.finish()


MIX_PIECES = 2


def mixer_exit(reads, out_proj, tokens, ffn_gain, branch_gate, route_ids, route_logits, size):
    count, width = tokens.shape
    part = width // size
    fast = fast_extent("tp", size)
    bf16 = jnp.bfloat16
    whole = pl.BlockSpec(memory_space=pltpu.VMEM)
    far = pl.BlockSpec(memory_space=pl.ANY)
    return pl.pallas_call(
        functools.partial(exit_kernel, size),
        out_shape=(
            jax.ShapeDtypeStruct((count, part), bf16),
            jax.ShapeDtypeStruct((count, part), bf16),
            jax.ShapeDtypeStruct((8, 128), jnp.float32),
        ),
        in_specs=[whole, far, far] + [whole] * 4,
        out_specs=(whole,) * 3,
        scratch_shapes=[
            pltpu.VMEM(out_proj.shape, bf16),
            pltpu.VMEM((count, part), bf16),
            pltpu.SemaphoreType.DMA((2,)),
            pltpu.VMEM((count, width), bf16),
            pltpu.VMEM((8, 128), jnp.float32),
            pltpu.VMEM((size - 1, 8, 128), jnp.float32),
            pltpu.SemaphoreType.DMA((size - 1,)),
            pltpu.SemaphoreType.DMA((size - 1,)),
        ]
        + reduce_scratch(fast, size // fast, count, part, MIX_PIECES),
        compiler_params=pltpu.CompilerParams(
            collective_id=0, has_side_effects=True, vmem_limit_bytes=58 << 20
        ),
    )(reads, out_proj, tokens, ffn_gain, branch_gate, route_ids, route_logits)


class Chain:
    def __init__(self, size):
        self.size = size
        self.x_size = fast_extent("ep", size)
        self.z_size = size // self.x_size
        self.me = lax.axis_index("ep")
        self.x = self.me % self.x_size
        self.z = self.me // self.x_size
        self.pending = []

    def at(self, j):
        left, right = self.z, self.z_size - 1 - self.z
        both = jnp.minimum(left, right)
        if j == 0:
            return self.z
        near = (j + 1) // 2
        paired = self.z - near if j % 2 else self.z + near
        single = jnp.where(left > right, self.z - (j - both), self.z + (j - both))
        return jnp.where(j <= 2 * both, paired, single)

    def index(self, z, x_step):
        return z * self.x_size + (self.x + x_step + self.x_size) % self.x_size

    def copy(self, source, target, sent, landed, peer):
        return pltpu.make_async_remote_copy(
            src_ref=source,
            dst_ref=target,
            send_sem=sent,
            recv_sem=landed,
            device_id={"ep": peer},
            device_id_type=MESH,
        )

    def launch(self, copy, cond=None):
        if cond is None:
            copy.start()
        else:
            pl.when(cond)(copy.start)
        self.pending.append((copy, cond))

    def finish(self):
        for copy, cond in self.pending:
            if cond is None:
                copy.wait_send()
            else:
                pl.when(cond)(copy.wait_send)


def layer_kernel(ep_size, tp_size, top, cap, names, *refs):
    own_cols, resid_cols, side = refs[:3]
    weights_hbm, out, refs = refs[3:9], refs[9], refs[10:]
    r = dict(zip(names, refs))
    extra = list(refs[len(names) :])
    f32, bf16 = jnp.float32, jnp.bfloat16
    chain, grid = Chain(ep_size), Grid("tp", tp_size)
    z_size, x_size, z, x = chain.z_size, chain.x_size, chain.z, chain.x
    rounds = ep_size // tp_size
    pieces = min(tp_size, 4)
    count, width = own_cols.shape

    def take(number):
        taken = extra[:number]
        del extra[:number]
        return taken

    dense_sums, hidden_gathers, row_gathers, expert_sums = [], [], [], []
    both, every_hidden, own_hidden, full, part = [], [], [], [], []
    for g in range(rounds):
        stores = take(5)
        for target, store in zip((both, every_hidden, own_hidden, full, part), stores):
            target.append(store)
        dense_sums.append(Reduce(grid, both[g], 1, False, take(8)))
        hidden_gathers.append(Gather(grid, own_hidden[g], every_hidden[g], 1, False, take(5)))
        row_gathers.append(
            Gather(grid, None, full[g], pieces, True, take(5), (tp_size * cap, width))
        )
        expert_sums.append(Reduce(grid, part[g], pieces, True, take(8)))

    near = [r[name] for name in WEIGHTS]
    loads = []
    for item, (source, target) in enumerate(zip(weights_hbm, near)):
        load = pltpu.make_async_copy(source, target, r["load_sems"].at[item])
        load.start()
        loads.append(load)
    dense_gate, dense_up, gate, up, down, dense_down = near
    barrier = pltpu.get_barrier_semaphore()
    for k in range(1, ep_size):
        pl.semaphore_signal(
            barrier, inc=1, device_id={"ep": (chain.me + k) % ep_size}, device_id_type=MESH
        )
    for k in range(1, tp_size):
        pl.semaphore_signal(
            barrier, inc=1, device_id={"tp": (grid.me + k) % tp_size}, device_id_type=MESH
        )
    pl.semaphore_wait(barrier, ep_size + tp_size - 2)

    cols, sides = r["cols"], r["sides"]

    def chunk(j, q=0):
        return chain.index(chain.at(j), -q)

    def send_chunk(j):
        spot = cols.at[chunk(j)]
        source = own_cols if j == 0 else spot
        at = chain.at(j)
        for turn, step, cond in (
            (0, 1, (at <= z) & (z < z_size - 1)),
            (1, -1, (at >= z) & (z > 0)),
        ):
            copy = chain.copy(
                source,
                spot,
                r["z_sent"].at[turn, j],
                r["z_landed"].at[at],
                jnp.where(cond, z + step, z) * x_size + x,
            )
            chain.launch(copy, cond)
        for q in range(1, x_size):
            copy = chain.copy(
                source,
                spot,
                r["x_sent"].at[q - 1, j],
                r["x_landed"].at[q - 1, j],
                chain.index(z, q),
            )
            chain.launch(copy)

    def wait_chunk(j, q):
        spot = cols.at[chunk(j, q)]
        if q:
            landed = r["x_landed"].at[q - 1, j]
        else:
            landed = r["z_landed"].at[chain.at(j)]
        chain.copy(spot, spot, r["x_sent"].at[0, 0], landed, chain.index(z, 1)).wait_recv()

    send_chunk(0)
    for k in range(1, ep_size):
        copy = chain.copy(
            side,
            sides.at[chain.me],
            r["side_sent"].at[k - 1],
            r["side_landed"].at[k - 1],
            (chain.me + k) % ep_size,
        )
        chain.launch(copy)

    mine = pl.ds(pl.multiple_of(grid.me * width, 128), width)
    hidden_width = dense_gate.shape[1]
    expert = chain.me.astype(f32)
    lane_ok = (lax.broadcasted_iota(jnp.int32, (1, 128), 1) < count).astype(f32)
    slots = lax.broadcasted_iota(jnp.int32, (128, 128), 0).astype(f32)
    before = (
        lax.broadcasted_iota(jnp.int32, (128, 128), 0)
        < lax.broadcasted_iota(jnp.int32, (128, 128), 1)
    ).astype(bf16)

    def process(j, q):
        i = j * x_size + q
        g, at = i // tp_size, i % tp_size
        if i == 0:
            block, info = own_cols[...], side[...]
        else:
            source = chunk(j, q)
            away = (chain.me - source + ep_size) % ep_size
            spot = sides.at[source]
            chain.copy(
                spot, spot, r["side_sent"].at[0], r["side_landed"].at[away - 1], source
            ).wait_recv()
            block, info = cols[source], sides[source]
        taken, weight = jnp.zeros((1, 128), f32), jnp.zeros((1, 128), f32)
        for item in range(top):
            hit = jnp.where(info[item : item + 1] == expert, lane_ok, 0.0)
            taken = taken + hit
            weight = weight + hit * info[top + item : top + item + 1]
        rank = jnp.dot(
            jnp.broadcast_to(taken, (8, 128)).astype(bf16), before, preferred_element_type=f32
        )[0:1]
        table = jnp.where(slots == rank, taken, 0.0)
        rows = jnp.dot(
            table[:cap, :count].astype(bf16), block, preferred_element_type=f32
        ).astype(bf16)
        full[g][at * cap : (at + 1) * cap, mine] = rows
        share = tp_size // pieces
        if at % share == share - 1:
            row_gathers[g].start_piece(at // share)
        r["turned"][i] = jnp.where(
            slots == 127.0, info[2 * top : 2 * top + 1], table * weight
        ).T
        if i == 0:
            loads[0].wait()
            loads[1].wait()
        both[g][at, :, :hidden_width] = jnp.dot(
            block, dense_gate[...], preferred_element_type=f32
        ).astype(bf16)
        both[g][at, :, hidden_width:] = jnp.dot(
            block, dense_up[...], preferred_element_type=f32
        ).astype(bf16)
        if at == tp_size - 1:
            dense_sums[g].push()
        if at == 0 and g > 0:
            dense_sums[g - 1].relay()

    inner = gate.shape[1]
    tile = tile_of(inner)
    hidden = r["hidden"]

    def expert_hidden(g):
        row_gathers[g].relay()
        row_gathers[g].arrive()
        rows = full[g]

        @pl.loop(0, inner // tile)
        def _(step):
            span = pl.ds(pl.multiple_of(step * tile, 128), tile)
            gate_val = jnp.dot(rows[...], gate[:, span], preferred_element_type=f32)
            up_val = jnp.dot(rows[...], up[:, span], preferred_element_type=f32)
            hidden[g, :, span] = (jax.nn.silu(gate_val) * up_val).astype(bf16)

    wide = tile_of(width)

    def expert_part(g):
        target = part[g]

        @pl.loop(0, tp_size * width // wide)
        def _(step):
            span = pl.ds(pl.multiple_of(step * wide, 128), wide)
            target[:, span] = jnp.dot(
                hidden[g], down[:, span], preferred_element_type=f32
            ).astype(bf16)

    def dense_hidden(g):
        def emit(span, value):
            own_hidden[g][span, :] = (
                jax.nn.silu(value[:, :hidden_width]) * value[:, hidden_width:]
            ).astype(bf16)

        dense_sums[g].collect(emit)
        hidden_gathers[g].start()

    for j in range(z_size):
        if j:
            wait_chunk(j, 0)
            send_chunk(j)
            for q in range(1, x_size):
                wait_chunk(j - 1, q)
                process(j - 1, q)
        process(j, 0)
    loads[2].wait()
    loads[3].wait()
    last = rounds - 1
    for g in range(last):
        expert_hidden(g)
    for q in range(1, x_size):
        wait_chunk(z_size - 1, q)
        process(z_size - 1, q)
    dense_sums[last].relay()
    for g in range(last):
        dense_hidden(g)
    loads[4].wait()
    for g in range(last):
        expert_part(g)
    expert_hidden(last)
    dense_hidden(last)
    expert_part(last)
    for g in reversed(range(rounds)):
        expert_sums[g].push()
        expert_sums[g].relay()
    for g in range(rounds):
        hidden_gathers[g].relay()
    for g in range(rounds):
        hidden_gathers[g].arrive()
    loads[5].wait()

    collected, own_share = set(), r["own_share"]

    def share_of(j, q):
        i = j * x_size + q
        g, at = i // tp_size, i % tp_size
        chunks = tp_size // pieces
        piece = at // chunks
        if (g, piece) not in collected:
            collected.add((g, piece))
            rows = chunks * cap
            r["expert_out"][g, piece * rows : (piece + 1) * rows, :] = (
                expert_sums[g].collect_piece(piece).astype(bf16)
            )
        turned = r["turned"][i]
        routed = jnp.dot(
            turned[:count, :cap].astype(bf16),
            r["expert_out"][g, at * cap : (at + 1) * cap, :],
            preferred_element_type=f32,
        )
        dense = jnp.dot(every_hidden[g][at], dense_down[...], preferred_element_type=f32)
        return routed + turned[:count, 127:128] * dense

    def send_share(j):
        for q in range(1, x_size):
            i = j * x_size + q
            r["x_share"][i] = share_of(j, q).astype(bf16)
            copy = chain.copy(
                r["x_share"].at[i],
                r["x_got"].at[j, q - 1],
                r["xs_sent"].at[i],
                r["xs_landed"].at[j, q - 1],
                chain.index(z, -q),
            )
            chain.launch(copy)
        own_share[j] = share_of(j, 0)

    def finish_share(j):
        for q in range(1, x_size):
            spot = r["x_got"].at[j, q - 1]
            chain.copy(
                spot, spot, r["xs_sent"].at[0], r["xs_landed"].at[j, q - 1], chain.index(z, q)
            ).wait_recv()
            own_share[j] = own_share[j] + r["x_got"][j, q - 1].astype(f32)
        at = chain.at(j)
        for turn, cond in (
            (0, (at <= z) & (z < z_size - 1)),
            (1, (at >= z) & (z > 0)),
        ):

            @pl.when(cond)
            def _():
                spot = r["z_got"].at[turn, at]
                chain.copy(
                    spot,
                    spot,
                    r["zs_sent"].at[0],
                    r["zs_landed"].at[turn, at],
                    chain.index(z, 1),
                ).wait_recv()
                own_share[j] = own_share[j] + r["z_got"][turn, at].astype(f32)

        if j == 0:
            total = own_share[0].astype(bf16).astype(f32)
            out[...] = (resid_cols[...].astype(f32) + total).astype(bf16)
        else:
            r["z_share"][j] = own_share[j].astype(bf16)
            turn = jnp.where(at < z, 0, 1)
            copy = chain.copy(
                r["z_share"].at[j],
                r["z_got"].at[turn, at],
                r["zs_sent"].at[j],
                r["zs_landed"].at[turn, at],
                jnp.where(at < z, z - 1, z + 1) * x_size + x,
            )
            chain.launch(copy)

    for j in reversed(range(z_size)):
        send_share(j)
        if j + 1 < z_size:
            finish_share(j + 1)
    finish_share(0)
    chain.finish()
    for phase in dense_sums + hidden_gathers + row_gathers + expert_sums:
        phase.finish()


WEIGHTS = ("dense_gate", "dense_up", "gate", "up", "down", "dense_down")


def layer(own_cols, resid_cols, side, weights, top, ep_size, tp_size):
    count, width = own_cols.shape
    bf16, f32 = jnp.bfloat16, jnp.float32
    vmem, dma = pltpu.VMEM, pltpu.SemaphoreType.DMA
    x_size = fast_extent("ep", ep_size)
    z_size = ep_size // x_size
    cap = max(2, 2 * count * top // ep_size)
    cap = -(-cap // 16) * 16
    hidden_width, inner = weights[0].shape[1], weights[2].shape[1]
    rounds, rows = ep_size // tp_size, tp_size * cap
    pieces = min(tp_size, 4)
    fast = fast_extent("tp", tp_size)
    slow = tp_size // fast
    named = {name: vmem(array.shape, bf16) for name, array in zip(WEIGHTS, weights)}
    named.update(
        load_sems=dma((len(weights),)),
        cols=vmem((ep_size, count, width), bf16),
        sides=vmem((ep_size, 8, 128), f32),
        turned=vmem((ep_size, 128, 128), f32),
        hidden=vmem((rounds, rows, inner), bf16),
        expert_out=vmem((rounds, rows, width), bf16),
        own_share=vmem((z_size, count, width), f32),
        x_share=vmem((ep_size, count, width), bf16),
        x_got=vmem((z_size, x_size - 1, count, width), bf16),
        z_share=vmem((z_size, count, width), bf16),
        z_got=vmem((2, z_size, count, width), bf16),
        z_sent=dma((2, z_size)),
        z_landed=dma((z_size,)),
        x_sent=dma((x_size - 1, z_size)),
        x_landed=dma((x_size - 1, z_size)),
        side_sent=dma((ep_size - 1,)),
        side_landed=dma((ep_size - 1,)),
        xs_sent=dma((ep_size,)),
        xs_landed=dma((z_size, x_size - 1)),
        zs_sent=dma((z_size,)),
        zs_landed=dma((2, z_size)),
    )
    extra = []
    for _ in range(rounds):
        extra += [
            vmem((tp_size, count, 2 * hidden_width), bf16),
            vmem((tp_size, count, hidden_width), bf16),
            vmem((count, hidden_width), bf16),
            vmem((rows, tp_size * width), bf16),
            vmem((rows, tp_size * width), bf16),
        ]
        extra += reduce_scratch(fast, slow, count, 2 * hidden_width, 1)
        extra += gather_sems(fast, slow, 1) + gather_sems(fast, slow, pieces)
        extra += reduce_scratch(fast, slow, rows, width, pieces)
    whole = pl.BlockSpec(memory_space=pltpu.VMEM)
    far = pl.BlockSpec(memory_space=pl.ANY)
    return pl.pallas_call(
        functools.partial(layer_kernel, ep_size, tp_size, top, cap, tuple(named)),
        out_shape=jax.ShapeDtypeStruct((count, width), bf16),
        in_specs=[whole] * 3 + [far] * len(weights),
        out_specs=whole,
        scratch_shapes=list(named.values()) + extra,
        compiler_params=pltpu.CompilerParams(
            collective_id=1, has_side_effects=True, vmem_limit_bytes=62 << 20
        ),
    )(own_cols, resid_cols, side, *weights)


def shards(
    tokens,
    mix_gain,
    ffn_gain,
    in_proj,
    decay_rate,
    frequency,
    log_step,
    b_real,
    b_imag,
    c_real,
    c_imag,
    skip_gain,
    states,
    out_proj,
    route_ids,
    route_logits,
    expert_gate,
    expert_up,
    expert_down,
    dense_gate,
    dense_up,
    dense_down,
    branch_gate,
):
    tp_count = lax.axis_size("tp")
    ep_count = lax.axis_size("ep")
    reads, new_states = mixer(
        tokens,
        mix_gain.reshape(1, -1),
        in_proj,
        decay_rate,
        frequency,
        log_step.reshape(1, -1),
        jnp.swapaxes(b_real, 1, 2),
        jnp.swapaxes(b_imag, 1, 2),
        c_real,
        c_imag,
        skip_gain.reshape(1, -1),
        states,
    )
    own_cols, resid_cols, side = mixer_exit(
        reads,
        out_proj,
        tokens,
        ffn_gain.reshape(1, -1),
        branch_gate.astype(jnp.float32).reshape(1, -1),
        route_ids.T,
        route_logits.T,
        tp_count,
    )
    weights = (dense_gate, dense_up, expert_gate[0], expert_up[0], expert_down[0], dense_down)
    output = layer(own_cols, resid_cols, side, weights, route_ids.shape[1], ep_count, tp_count)
    return (output, new_states)


def solution(mesh):
    return jax.shard_map(
        shards,
        mesh=mesh,
        in_specs=(
            P("ep", None),
            P(),
            P(),
            P(None, "tp"),
            P("tp", None),
            P("tp", None),
            P("tp"),
            P("tp", None, None),
            P("tp", None, None),
            P("tp", None, None),
            P("tp", None, None),
            P("tp"),
            P(None, "ep", "tp"),
            P("tp", None),
            P("ep", None),
            P("ep", None),
            P("ep", None, "tp"),
            P("ep", None, "tp"),
            P("ep", "tp", None),
            P("tp", "ep"),
            P("tp", "ep"),
            P("ep", "tp"),
            P(),
        ),
        out_specs=(P("ep", "tp"), P(None, "ep", "tp")),
        check_vma=False,
    )
```

time: 152 us -> 112 us (0.74)
  Pallas kernels: 131 us -> 108 us
  local copies, waits for them, and re-layouts: 12.3 us -> 1.62 us
  matrix products: 5.39 us -> 0 us
    pallas_call x4 -> x2, Pallas kernels: 117 us -> 92.8 us  [the longest x1 87.2 us: layer(): pl.pallas_call(functools.partial(layer_kernel, ep_size, tp_size, top, cap...]
    unnamed x34 -> x1, local copies, waits for them, and re-layouts: 11.8 us -> 1.62 us
    dot_general x3 -> x0, matrix products: 5.39 us -> none  [the longest x1 2.33 us: shards(): lax.dot_general(select, weighted, (((0,), (0,)), ((), ())), preferred_ele...]
    pallas_call x1, Pallas kernels: 13.9 us -> 15.5 us  [mixer_exit(): pl.pallas_call(functools.partial(exit_kernel, size), out_shape=(jax.Shape...]
where the time goes in v2:
time: 112 us
  Pallas kernels  108 us (96%)
  local copies, waits for them, and re-layouts  1.62 us (1%)
  other arithmetic  1.3 us (1%)
    pallas_call x1, Pallas kernels, layer(): pl.pallas_call(functools.partial(layer_kernel, ep_size, tp_size, top, cap...  87.2 us
    pallas_call x1, Pallas kernels, mixer_exit(): pl.pallas_call(functools.partial(exit_kernel, size), out_shape=(jax.Shape...  15.5 us
    pallas_call x1, Pallas kernels, mixer(): pl.pallas_call(mixer_kernel, out_shape=(jax.ShapeDtypeStruct((tokens.shap...  5.64 us

profile of v2, /device:TPU:0, one launch (start us, length us, event | category | flops | bytes accessed | tf_op | source)
XLA Modules:
  0.0 111.9 jit_solution(93892645005994590)
XLA Ops:
  0.6 1.3 %reshape.27 = f32[4096]{0:T(1024)} convert(bf16[4096]{0:T(1024)(128)(2,1)} %param.45) | non-fusion elementwise | flops 4096 | bytes 24576 | tf_op jit(solution)/shard_map/reshape | solution.py:974
  1.9 5.6 %shard_map.230 = (bf16[96,256]{1,0:T(8,128)(2,1)}, f32[2,96,1024]{2,1,0:T(8,128)}) custom-call(bf16[96,4096]{1,0:T(8,128)(2,1)} %tokens_hbm.1, f32[1,4096]{1,0:T(1,128)} %bitcast.18, bf16[4096,256]{1,0:T(8,128)(2,1)} %refs_2_.1, f32[16,64]{1,0:T(8,128)} %refs_3_.2, f32[16,64]{1,0:T(8,128)} %refs_4_.2, f32[1,16]{1,0:T(1,128)} %bitcast.23, ...), custom_call_target="tpu_custom_call" | custom-call | tf_op jit(solution)/shard_map/pallas_call | solution.py:346
  7.6 15.5 %shard_map.231 = (bf16[96,1024]{1,0:T(8,128)(2,1)}, bf16[96,1024]{1,0:T(8,128)(2,1)}, f32[8,128]{1,0:T(8,128)}) custom-call(bf16[96,256]{1,0:T(8,128)(2,1)} %get-tuple-element.7.reads, bf16[256,4096]{1,0:T(8,128)(2,1)} %out_proj_hbm.1, bf16[96,4096]{1,0:T(8,128)(2,1)} %tokens_hbm.1, f32[1,4096]{1,0:T(1,128)} %bitcast.19, f32[1,4096]{1,0:T(1,128)} %bitcast.17, ...), custom_call_target="tpu_custom_call" | custom-call | tf_op jit(solution)/shard_map/pallas_call | solution.py:477
  23.1 87.2 %shard_map.232 = bf16[96,1024]{1,0:T(8,128)(2,1)} custom-call(bf16[96,1024]{1,0:T(8,128)(2,1)} %get-tuple-element.8.refs_0_, bf16[96,1024]{1,0:T(8,128)(2,1)} %get-tuple-element.9.refs_1_, f32[8,128]{1,0:T(8,128)} %get-tuple-element.10.refs_2_, bf16[1024,768]{1,0:T(8,128)(2,1)} %refs_3_.3, bf16[1024,768]{1,0:T(8,128)(2,1)} %refs_4_.3, ...), custom_call_target="tpu_custom_call" | custom-call | tf_op jit(solution)/shard_map/pallas_call | solution.py:916
  110.3 1.6 %copy.26 = bf16[96,1024]{1,0:T(8,128)(2,1)} copy(bf16[96,1024]{1,0:T(8,128)(2,1)} %shard_map.232) | data formatting | bytes 393216

commit v3 on v2

--- a/solution.py
+++ b/solution.py
@@ -38,24 +38,6 @@
         return [self.index(k, 0) for k in range(1, self.slow)] + [
             self.index(0, q) for q in range(1, self.fast)
         ]
-
-    def greet(self):
-        barrier = pltpu.get_barrier_semaphore()
-        peers = self.peers()
-        for peer in peers:
-            pl.semaphore_signal(barrier, inc=1, device_id={self.axis: peer}, device_id_type=MESH)
-        pl.semaphore_wait(barrier, len(peers))
-
-    def greet_all(self):
-        barrier = pltpu.get_barrier_semaphore()
-        for k in range(1, self.size):
-            pl.semaphore_signal(
-                barrier,
-                inc=1,
-                device_id={self.axis: (self.me + k) % self.size},
-                device_id_type=MESH,
-            )
-        pl.semaphore_wait(barrier, self.size - 1)
 
     def copy(self, source, target, sent, landed, peer):
         return pltpu.make_async_remote_copy(
@@ -193,7 +175,7 @@
 
     def push_part(self, k, q):
         grid = self.grid
-        for j in range(self.number):
+        for j in reversed(range(self.number)):
             copy = self.fast_copy(self.part(grid.index(k, q), j), k, j, q, grid.index(0, q))
             copy.start()
             self.pending.append(copy)
@@ -203,10 +185,10 @@
             for q in range(1, self.grid.fast):
                 self.push_part(k, q)
 
-    def relay(self):
+    def relay(self, pieces=None):
         grid = self.grid
         for k in range(1, grid.slow + 1):
-            for j in range(self.number):
+            for j in reversed(range(self.number) if pieces is None else pieces):
                 value = self.part(grid.index(k, 0), j)[...].astype(jnp.float32)
                 for q in range(1, grid.fast):
                     block = self.got_fast.at[q - 1, k - 1, self.span(j), :]
@@ -259,15 +241,15 @@
 def mixer_kernel(
     *refs,
 ):
-    far, reads, fresh_hbm = refs[:12], refs[12], refs[13]
-    near, fresh, normed, sems = refs[14:26], refs[26], refs[27], refs[28]
+    far, partial, fresh_hbm = refs[:13], refs[13], refs[14]
+    near, fresh, normed, sems = refs[15:28], refs[28], refs[29], refs[30]
     loads = []
     for item, (source, target) in enumerate(zip(far, near)):
         load = pltpu.make_async_copy(source, target, sems.at[item])
         load.start()
         loads.append(load)
     tokens, mix_gain, in_proj, decay_rate, frequency, log_step = near[:6]
-    b_real, b_imag, c_real, c_imag, skip_gain, old = near[6:]
+    b_real, b_imag, c_real, c_imag, skip_gain, old, out_proj = near[6:]
     count, width = tokens.shape
     groups, entries = decay_rate.shape
     channels = skip_gain.shape[1]
@@ -320,7 +302,7 @@
         normed[start : start + step, :] = (flt * scale * mix_gain[...]).astype(bf16)
     loads[2].wait()
     drive = jnp.dot(normed[...], in_proj[...], preferred_element_type=f32).astype(bf16)
-    for load in loads[6:]:
+    for load in loads[6:12]:
         load.wait()
     push_a = jnp.dot(drive, matrix(b_real), preferred_element_type=f32)
     push_b = jnp.dot(drive, matrix(b_imag), preferred_element_type=f32)
@@ -329,24 +311,30 @@
     fresh[0] = new_re
     new_im = abar_re * old_im + abar_im * old_re + fac_re * push_b + fac_im * push_a
     fresh[1] = new_im
-    store = pltpu.make_async_copy(fresh, fresh_hbm, sems.at[12])
+    store = pltpu.make_async_copy(fresh, fresh_hbm, sems.at[13])
     store.start()
     readout = (
         by_rows(new_re.astype(bf16), matrix(c_real))
         - by_rows(new_im.astype(bf16), matrix(c_imag))
         + skip_gain[...] * drive.astype(f32)
     )
-    reads[...] = jax.nn.gelu(readout).astype(bf16)
+    reads = jax.nn.gelu(readout).astype(bf16)
+    loads[12].wait()
+    span = min(1024, partial.shape[1])
+    for start in range(0, partial.shape[1], span):
+        partial[:, start : start + span] = jnp.dot(
+            reads, out_proj[:, start : start + span], preferred_element_type=f32
+        ).astype(bf16)
     store.wait()
 
 
 def mixer(*arrays):
-    tokens, in_proj, states = arrays[0], arrays[2], arrays[-1]
+    tokens, states = arrays[0], arrays[-2]
     far = pl.BlockSpec(memory_space=pl.ANY)
     return pl.pallas_call(
         mixer_kernel,
         out_shape=(
-            jax.ShapeDtypeStruct((tokens.shape[0], in_proj.shape[1]), jnp.bfloat16),
+            jax.ShapeDtypeStruct(tokens.shape, jnp.bfloat16),
             jax.ShapeDtypeStruct(states.shape, jnp.float32),
         ),
         in_specs=[far] * len(arrays),
@@ -355,149 +343,10 @@
         + [
             pltpu.VMEM(states.shape, jnp.float32),
             pltpu.VMEM(tokens.shape, jnp.bfloat16),
-            pltpu.SemaphoreType.DMA((13,)),
+            pltpu.SemaphoreType.DMA((14,)),
         ],
         compiler_params=pltpu.CompilerParams(vmem_limit_bytes=62 << 20),
     )(*arrays)
-
-
-def exit_kernel(
-    size,
-    reads,
-    out_proj_hbm,
-    tokens_hbm,
-    ffn_gain,
-    branch_gate,
-    route_ids,
-    route_logits,
-    own_cols,
-    resid_cols,
-    side,
-    out_proj,
-    tokens,
-    load_sems,
-    partial,
-    stat,
-    stat_got,
-    stat_sent,
-    stat_landed,
-    *scratch,
-):
-    f32, bf16 = jnp.float32, jnp.bfloat16
-    grid = Grid("tp", size)
-    mix = Reduce(grid, partial, MIX_PIECES, True, scratch)
-    count, width = resid_cols.shape
-    mine = pl.ds(pl.multiple_of(grid.me * width, 128), width)
-    loads = [
-        pltpu.make_async_copy(out_proj_hbm, out_proj, load_sems.at[0]),
-        pltpu.make_async_copy(tokens_hbm.at[:, mine], tokens, load_sems.at[1]),
-    ]
-    for load in loads:
-        load.start()
-    grid.greet_all()
-    for load in loads:
-        load.wait()
-
-    def block(dest):
-        span = pl.ds(pl.multiple_of(dest * width, 128), width)
-        partial[:, span] = jnp.dot(
-            reads[...], out_proj[:, span], preferred_element_type=f32
-        ).astype(bf16)
-
-    for k in range(1, grid.slow + 1):
-        for q in range(1, grid.fast):
-            block(grid.index(k, q))
-            mix.push_part(k, q)
-    for k in range(1, grid.slow + 1):
-        block(grid.index(k, 0))
-    logits = route_logits[...]
-    top = logits.shape[0]
-    raised = jnp.exp(logits - jnp.max(logits, axis=0, keepdims=True))
-    weights = raised / jnp.sum(raised, axis=0, keepdims=True)
-    side[...] = jnp.zeros((8, 128), f32)
-    side[0:top, 0:count] = route_ids[...].astype(f32)
-    side[top : 2 * top, 0:count] = weights
-    mix.relay()
-    gain = ffn_gain[:, mine]
-    gate = gain * branch_gate[:, mine]
-    lanes = lax.broadcasted_iota(jnp.int32, (count, 128), 1)
-    ssq_parts, dot_parts = [], []
-
-    def emit(span, value):
-        mixed = value.astype(bf16).astype(f32)
-        resid = (tokens[span, :].astype(f32) + mixed).astype(bf16)
-        resid_cols[span, :] = resid
-        flt = resid.astype(f32)
-        ssq_parts.append(jnp.sum(flt * flt, axis=1, keepdims=True))
-        dot_parts.append(jnp.sum(flt * gate, axis=1, keepdims=True))
-
-    mix.collect(emit)
-    ssq, dots = jnp.concatenate(ssq_parts, axis=0), jnp.concatenate(dot_parts, axis=0)
-    table = jnp.where(lanes == 0, ssq, jnp.where(lanes == 1, dots, 0.0))
-    if count < 128:
-        table = jnp.concatenate([table, jnp.zeros((128 - count, 128), f32)], axis=0)
-    turned = table.T
-    stat[...] = turned[:8]
-    copies = []
-    for k in range(1, size):
-        copy = grid.copy(
-            stat,
-            stat_got.at[k - 1],
-            stat_sent.at[k - 1],
-            stat_landed.at[k - 1],
-            (grid.me + k) % size,
-        )
-        copy.start()
-        copies.append(copy)
-    total = turned[:8]
-    for copy in copies:
-        copy.wait_recv()
-    for k in range(1, size):
-        total = total + stat_got[k - 1]
-    scale = lax.rsqrt(total[0:1] / (width * size) + 1e-06)
-    branch = jax.nn.sigmoid(total[1:2] * scale)
-    side[2 * top : 2 * top + 1, :] = branch
-    column = jnp.broadcast_to(scale, (128, 128)).T[:count, 0:1]
-    own_cols[...] = (resid_cols[...].astype(f32) * column * gain).astype(bf16)
-    for copy in copies:
-        copy.wait_send()
-    mix.finish()
-
-
-MIX_PIECES = 2
-
-
-def mixer_exit(reads, out_proj, tokens, ffn_gain, branch_gate, route_ids, route_logits, size):
-    count, width = tokens.shape
-    part = width // size
-    fast = fast_extent("tp", size)
-    bf16 = jnp.bfloat16
-    whole = pl.BlockSpec(memory_space=pltpu.VMEM)
-    far = pl.BlockSpec(memory_space=pl.ANY)
-    return pl.pallas_call(
-        functools.partial(exit_kernel, size),
-        out_shape=(
-            jax.ShapeDtypeStruct((count, part), bf16),
-            jax.ShapeDtypeStruct((count, part), bf16),
-            jax.ShapeDtypeStruct((8, 128), jnp.float32),
-        ),
-        in_specs=[whole, far, far] + [whole] * 4,
-        out_specs=(whole,) * 3,
-        scratch_shapes=[
-            pltpu.VMEM(out_proj.shape, bf16),
-            pltpu.VMEM((count, part), bf16),
-            pltpu.SemaphoreType.DMA((2,)),
-            pltpu.VMEM((count, width), bf16),
-            pltpu.VMEM((8, 128), jnp.float32),
-            pltpu.VMEM((size - 1, 8, 128), jnp.float32),
-            pltpu.SemaphoreType.DMA((size - 1,)),
-            pltpu.SemaphoreType.DMA((size - 1,)),
-        ]
-        + reduce_scratch(fast, size // fast, count, part, MIX_PIECES),
-        compiler_params=pltpu.CompilerParams(
-            collective_id=0, has_side_effects=True, vmem_limit_bytes=58 << 20
-        ),
-    )(reads, out_proj, tokens, ffn_gain, branch_gate, route_ids, route_logits)
 
 
 class Chain:
@@ -520,6 +369,14 @@
         single = jnp.where(left > right, self.z - (j - both), self.z + (j - both))
         return jnp.where(j <= 2 * both, paired, single)
 
+    def traced_at(self, j):
+        left, right = self.z, self.z_size - 1 - self.z
+        both = jnp.minimum(left, right)
+        near = (j + 1) // 2
+        paired = jnp.where(j % 2 == 1, self.z - near, self.z + near)
+        single = jnp.where(left > right, self.z - (j - both), self.z + (j - both))
+        return jnp.where(j <= 2 * both, paired, single)
+
     def index(self, z, x_step):
         return z * self.x_size + (self.x + x_step + self.x_size) % self.x_size
 
@@ -549,10 +406,12 @@
 
 
 def layer_kernel(ep_size, tp_size, top, cap, names, *refs):
-    own_cols, resid_cols, side = refs[:3]
-    weights_hbm, out, refs = refs[3:9], refs[9], refs[10:]
+    partial, ffn_gain, route_ids, route_logits = refs[:4]
+    weights_hbm, branch_hbm, tokens_hbm = refs[4:10], refs[10], refs[11]
+    out, resid_cols, refs = refs[12], refs[13], refs[14:]
     r = dict(zip(names, refs))
     extra = list(refs[len(names) :])
+    own_cols, side, late = r["own_cols"], r["side"], r["late"]
     f32, bf16 = jnp.float32, jnp.bfloat16
     chain, grid = Chain(ep_size), Grid("tp", tp_size)
     z_size, x_size, z, x = chain.z_size, chain.x_size, chain.z, chain.x
@@ -578,75 +437,154 @@
         )
         expert_sums.append(Reduce(grid, part[g], pieces, True, take(8)))
 
+    mix = Reduce(grid, partial, PIECES, True, take(8))
+    mine = pl.ds(pl.multiple_of(grid.me * width, 128), width)
     near = [r[name] for name in WEIGHTS]
     loads = []
-    for item, (source, target) in enumerate(zip(weights_hbm, near)):
+    transfers = list(zip(weights_hbm, near))
+    transfers.insert(0, (tokens_hbm.at[:, mine], r["tokens"]))
+    transfers.insert(1, (branch_hbm.at[mine], r["branch"]))
+    for item, (source, target) in enumerate(transfers):
         load = pltpu.make_async_copy(source, target, r["load_sems"].at[item])
         load.start()
         loads.append(load)
+    first_loads, loads = loads[:2], loads[2:]
     dense_gate, dense_up, gate, up, down, dense_down = near
     barrier = pltpu.get_barrier_semaphore()
-    for k in range(1, ep_size):
+    for k in range(1, x_size):
         pl.semaphore_signal(
-            barrier, inc=1, device_id={"ep": (chain.me + k) % ep_size}, device_id_type=MESH
-        )
+            barrier, inc=1, device_id={"ep": chain.index(z, k)}, device_id_type=MESH
+        )
+    ends = (z > 0, z - 1), (z < z_size - 1, z + 1)
+    for cond, at in ends:
+
+        @pl.when(cond)
+        def _():
+            pl.semaphore_signal(
+                barrier, inc=1, device_id={"ep": at * x_size + x}, device_id_type=MESH
+            )
     for k in range(1, tp_size):
         pl.semaphore_signal(
             barrier, inc=1, device_id={"tp": (grid.me + k) % tp_size}, device_id_type=MESH
         )
-    pl.semaphore_wait(barrier, ep_size + tp_size - 2)
-
-    cols, sides = r["cols"], r["sides"]
+    beside = (z + z_size - 1) // z_size + (2 * z_size - 2 - z) // z_size
+    pl.semaphore_wait(barrier, x_size + tp_size - 2 + beside)
+    mix.push()
+    logits = route_logits[...]
+    raised = jnp.exp(logits - jnp.max(logits, axis=0, keepdims=True))
+    side[...] = jnp.zeros((8, 128), f32)
+    late[...] = jnp.zeros((8, 128), f32)
+    side[0:top, 0:count] = route_ids[...].astype(f32)
+    side[top : 2 * top, 0:count] = raised / jnp.sum(raised, axis=0, keepdims=True)
+    for load in first_loads:
+        load.wait()
+    mix.relay()
+
+    cols, sides, lates = r["cols"], r["sides"], r["lates"]
 
     def chunk(j, q=0):
         return chain.index(chain.at(j), -q)
 
-    def send_chunk(j):
-        spot = cols.at[chunk(j)]
-        source = own_cols if j == 0 else spot
+    step = count // PIECES
+
+    def spot_of(source, p):
+        if p >= PIECES:
+            return (sides, lates)[p - PIECES].at[source]
+        return cols.at[source, pl.ds(p * step, step), :]
+
+    def chunk_of(j, q):
+        return chain.index(chain.traced_at(j), -q)
+
+    def send_chunk(j, p, cond=None, record=True, along=True, across=True):
         at = chain.at(j)
-        for turn, step, cond in (
+        spot = spot_of(chunk(j), p)
+        if j:
+            source = spot
+        else:
+            source = (side, late)[p - PIECES] if p >= PIECES else own_cols.at[pl.ds(p * step, step), :]
+        copies = []
+        for turn, move, go in (
             (0, 1, (at <= z) & (z < z_size - 1)),
             (1, -1, (at >= z) & (z > 0)),
-        ):
+        ) if along else ():
             copy = chain.copy(
                 source,
                 spot,
-                r["z_sent"].at[turn, j],
-                r["z_landed"].at[at],
-                jnp.where(cond, z + step, z) * x_size + x,
+                r["z_sent"].at[turn, j, p],
+                r["z_landed"].at[at, p],
+                jnp.where(go, z + move, z) * x_size + x,
             )
-            chain.launch(copy, cond)
-        for q in range(1, x_size):
+            copies.append((copy, go))
+        for q in range(1, x_size) if across else ():
             copy = chain.copy(
                 source,
                 spot,
-                r["x_sent"].at[q - 1, j],
-                r["x_landed"].at[q - 1, j],
+                r["x_sent"].at[q - 1, j, p],
+                r["x_landed"].at[q - 1, j, p],
                 chain.index(z, q),
             )
-            chain.launch(copy)
+            copies.append((copy, None))
+        for copy, go in copies:
+            if go is None:
+                copy.start() if cond is None else pl.when(cond)(copy.start)
+            else:
+                pl.when(go if cond is None else go & cond)(copy.start)
+            if record:
+                chain.pending.append((copy, go))
+
+    def wait_piece(j, q, p):
+        spot = spot_of(chunk(j, q), p)
+        if q:
+            landed = r["x_landed"].at[q - 1, j, p]
+        else:
+            landed = r["z_landed"].at[chain.at(j), p]
+        chain.copy(spot, spot, r["x_sent"].at[0, 0, 0], landed, chain.index(z, 1)).wait_recv()
 
     def wait_chunk(j, q):
-        spot = cols.at[chunk(j, q)]
-        if q:
-            landed = r["x_landed"].at[q - 1, j]
-        else:
-            landed = r["z_landed"].at[chain.at(j)]
-        chain.copy(spot, spot, r["x_sent"].at[0, 0], landed, chain.index(z, 1)).wait_recv()
-
-    send_chunk(0)
-    for k in range(1, ep_size):
-        copy = chain.copy(
-            side,
-            sides.at[chain.me],
-            r["side_sent"].at[k - 1],
-            r["side_landed"].at[k - 1],
-            (chain.me + k) % ep_size,
-        )
-        chain.launch(copy)
-
-    mine = pl.ds(pl.multiple_of(grid.me * width, 128), width)
+        for p in PARTS:
+            wait_piece(j, q, p)
+
+    gain = ffn_gain[:, mine]
+    gate_row = gain * r["branch"][...].astype(f32).reshape(1, width)
+    lanes = lax.broadcasted_iota(jnp.int32, (count, 128), 1)
+    tables = []
+    send_chunk(0, PIECES)
+    for p in reversed(range(PIECES)):
+        span = mix.span(p)
+        mixed = mix.collect_piece(p).astype(bf16).astype(f32)
+        resid = (r["tokens"][span, :].astype(f32) + mixed).astype(bf16)
+        resid_cols[span, :] = resid
+        flt = resid.astype(f32)
+        own_cols[span, :] = (flt * gain).astype(bf16)
+        send_chunk(0, p)
+        ssq = jnp.sum(flt * flt, axis=1, keepdims=True)
+        dots = jnp.sum(flt * gate_row, axis=1, keepdims=True)
+        tables.insert(0, jnp.where(lanes[:step] == 0, ssq, jnp.where(lanes[:step] == 1, dots, 0.0)))
+    if count < 128:
+        tables.append(jnp.zeros((128 - count, 128), f32))
+    stat = jnp.concatenate(tables, axis=0).T[:8]
+    r["stat"][...] = stat
+    copies = []
+    for k in range(1, tp_size):
+        copy = grid.copy(
+            r["stat"],
+            r["stat_got"].at[k - 1],
+            r["stat_sent"].at[k - 1],
+            r["stat_landed"].at[k - 1],
+            (grid.me + k) % tp_size,
+        )
+        copy.start()
+        copies.append(copy)
+
+    def finish_stat(stat=stat):
+        for k, copy in enumerate(copies):
+            copy.wait_recv()
+            stat = stat + r["stat_got"][k]
+        scale = lax.rsqrt(stat[0:1] / (width * tp_size) + 1e-06)
+        late[0:1, :] = jax.nn.sigmoid(stat[1:2] * scale)
+        late[1:2, :] = scale
+        lates[chain.me] = late[...]
+        send_chunk(0, PIECES + 1)
     hidden_width = dense_gate.shape[1]
     expert = chain.me.astype(f32)
     lane_ok = (lax.broadcasted_iota(jnp.int32, (1, 128), 1) < count).astype(f32)
@@ -663,11 +601,6 @@
             block, info = own_cols[...], side[...]
         else:
             source = chunk(j, q)
-            away = (chain.me - source + ep_size) % ep_size
-            spot = sides.at[source]
-            chain.copy(
-                spot, spot, r["side_sent"].at[0], r["side_landed"].at[away - 1], source
-            ).wait_recv()
             block, info = cols[source], sides[source]
         taken, weight = jnp.zeros((1, 128), f32), jnp.zeros((1, 128), f32)
         for item in range(top):
@@ -680,14 +613,13 @@
         table = jnp.where(slots == rank, taken, 0.0)
         rows = jnp.dot(
             table[:cap, :count].astype(bf16), block, preferred_element_type=f32
-        ).astype(bf16)
-        full[g][at * cap : (at + 1) * cap, mine] = rows
+        )
+        full[g][at * cap : (at + 1) * cap, mine] = rows.astype(bf16)
         share = tp_size // pieces
         if at % share == share - 1:
             row_gathers[g].start_piece(at // share)
-        r["turned"][i] = jnp.where(
-            slots == 127.0, info[2 * top : 2 * top + 1], table * weight
-        ).T
+        r["table"][i] = table
+        r["turned"][i] = (table * weight).T
         if i == 0:
             loads[0].wait()
             loads[1].wait()
@@ -708,17 +640,25 @@
 
     def expert_hidden(g):
         row_gathers[g].relay()
+        for at in range(tp_size):
+            i = g * tp_size + at
+            row = lates[chunk(i // x_size, i % x_size), 1:2, :]
+            scales = jnp.sum(r["table"][i] * row, axis=1, keepdims=True)
+            r["row_scale"][g, at * cap : (at + 1) * cap, :] = jnp.broadcast_to(
+                scales[:cap], (cap, 128)
+            )
         row_gathers[g].arrive()
         rows = full[g]
 
         @pl.loop(0, inner // tile)
         def _(step):
             span = pl.ds(pl.multiple_of(step * tile, 128), tile)
-            gate_val = jnp.dot(rows[...], gate[:, span], preferred_element_type=f32)
-            up_val = jnp.dot(rows[...], up[:, span], preferred_element_type=f32)
+            scale = r["row_scale"][g, :, 0:1]
+            gate_val = jnp.dot(rows[...], gate[:, span], preferred_element_type=f32) * scale
+            up_val = jnp.dot(rows[...], up[:, span], preferred_element_type=f32) * scale
             hidden[g, :, span] = (jax.nn.silu(gate_val) * up_val).astype(bf16)
 
-    wide = tile_of(width)
+    wide = min(WIDE, width)
 
     def expert_part(g):
         target = part[g]
@@ -731,42 +671,79 @@
             ).astype(bf16)
 
     def dense_hidden(g):
+        i = g * tp_size + grid.me
+        source = chunk_of(i // x_size, i % x_size)
+        turned = jnp.concatenate([lates[source], jnp.zeros((120, 128), f32)], axis=0).T[:count]
+        branch, scale = turned[:, 0:1], turned[:, 1:2]
+
         def emit(span, value):
+            value = value * scale
             own_hidden[g][span, :] = (
-                jax.nn.silu(value[:, :hidden_width]) * value[:, hidden_width:]
+                branch * jax.nn.silu(value[:, :hidden_width]) * value[:, hidden_width:]
             ).astype(bf16)
 
         dense_sums[g].collect(emit)
         hidden_gathers[g].start()
 
-    for j in range(z_size):
-        if j:
-            wait_chunk(j, 0)
-            send_chunk(j)
-            for q in range(1, x_size):
-                wait_chunk(j - 1, q)
-                process(j - 1, q)
+    fewer = jnp.minimum(z, z_size - 1 - z)
+
+    def pass_on(j, p, cond=None, record=True, **kinds):
+        def wait():
+            wait_piece(j, 0, p)
+
+        wait() if cond is None else pl.when(cond)(wait)
+        send_chunk(j, p, cond, record, **kinds)
+
+    last = rounds - 1
+    end = z_size - 1
+    process(0, 0)
+    finish_stat()
+    for j in range(1, end):
+        if j % 2:
+            two = j + 1 < end
+            paired = j + 1 <= 2 * fewer
+            for p in PARTS:
+                pass_on(j, p)
+                if two:
+                    pass_on(j + 1, p, paired, across=False)
+            if two:
+                for p in PARTS:
+                    send_chunk(j + 1, p, paired, along=False)
+        else:
+            for p in PARTS:
+                pass_on(j, p, j > 2 * fewer, False)
+        for q in range(1, x_size):
+            wait_chunk(j - 1, q)
+            process(j - 1, q)
         process(j, 0)
-    loads[2].wait()
-    loads[3].wait()
-    last = rounds - 1
+    for p in PARTS:
+        pass_on(end, p, fewer > 0)
+    for q in range(1, x_size):
+        wait_chunk(end - 1, q)
+        process(end - 1, q)
+    for load in loads[2:5]:
+        load.wait()
     for g in range(last):
         expert_hidden(g)
-    for q in range(1, x_size):
-        wait_chunk(z_size - 1, q)
-        process(z_size - 1, q)
-    dense_sums[last].relay()
+    for p in PARTS:
+        pass_on(end, p, fewer == 0, False)
+    process(end, 0)
     for g in range(last):
         dense_hidden(g)
-    loads[4].wait()
-    for g in range(last):
         expert_part(g)
+        expert_sums[g].push()
+    for q in range(1, x_size):
+        wait_chunk(end, q)
+        process(end, q)
+    dense_sums[last].relay()
+    expert_sums[0].relay(range(pieces // 2))
     expert_hidden(last)
+    expert_part(last)
+    expert_sums[last].push()
     dense_hidden(last)
-    expert_part(last)
-    for g in reversed(range(rounds)):
-        expert_sums[g].push()
+    for g in reversed(range(1, rounds)):
         expert_sums[g].relay()
+    expert_sums[0].relay(range(pieces // 2, pieces))
     for g in range(rounds):
         hidden_gathers[g].relay()
     for g in range(rounds):
@@ -793,30 +770,42 @@
             preferred_element_type=f32,
         )
         dense = jnp.dot(every_hidden[g][at], dense_down[...], preferred_element_type=f32)
-        return routed + turned[:count, 127:128] * dense
+        return routed + dense
 
     def send_share(j):
+        own_share[j] = share_of(j, 0)
+
+    def send_twins(j):
         for q in range(1, x_size):
             i = j * x_size + q
             r["x_share"][i] = share_of(j, q).astype(bf16)
-            copy = chain.copy(
-                r["x_share"].at[i],
-                r["x_got"].at[j, q - 1],
-                r["xs_sent"].at[i],
-                r["xs_landed"].at[j, q - 1],
-                chain.index(z, -q),
-            )
-            chain.launch(copy)
-        own_share[j] = share_of(j, 0)
+            for p in range(PIECES):
+                span = pl.ds(p * step, step)
+                copy = chain.copy(
+                    r["x_share"].at[i, span, :],
+                    r["x_got"].at[j, q - 1, span, :],
+                    r["xs_sent"].at[i, p],
+                    r["xs_landed"].at[j, q - 1, p],
+                    chain.index(z, -q),
+                )
+                chain.launch(copy)
 
     def finish_share(j):
+        at = chain.at(j)
+        for p in range(PIECES):
+            finish_piece(j, at, pl.ds(p * step, step), p)
+
+    def finish_piece(j, at, span, p):
         for q in range(1, x_size):
-            spot = r["x_got"].at[j, q - 1]
+            spot = r["x_got"].at[j, q - 1, span, :]
             chain.copy(
-                spot, spot, r["xs_sent"].at[0], r["xs_landed"].at[j, q - 1], chain.index(z, q)
+                spot,
+                spot,
+                r["xs_sent"].at[0, 0],
+                r["xs_landed"].at[j, q - 1, p],
+                chain.index(z, q),
             ).wait_recv()
-            own_share[j] = own_share[j] + r["x_got"][j, q - 1].astype(f32)
-        at = chain.at(j)
+            own_share[j, span, :] = own_share[j, span, :] + r["x_got"][j, q - 1, span, :].astype(f32)
         for turn, cond in (
             (0, (at <= z) & (z < z_size - 1)),
             (1, (at >= z) & (z > 0)),
@@ -824,46 +813,54 @@
 
             @pl.when(cond)
             def _():
-                spot = r["z_got"].at[turn, at]
+                spot = r["z_got"].at[turn, at, span, :]
                 chain.copy(
                     spot,
                     spot,
-                    r["zs_sent"].at[0],
-                    r["zs_landed"].at[turn, at],
+                    r["zs_sent"].at[0, 0],
+                    r["zs_landed"].at[turn, at, p],
                     chain.index(z, 1),
                 ).wait_recv()
-                own_share[j] = own_share[j] + r["z_got"][turn, at].astype(f32)
+                own_share[j, span, :] = own_share[j, span, :] + r["z_got"][
+                    turn, at, span, :
+                ].astype(f32)
 
         if j == 0:
-            total = own_share[0].astype(bf16).astype(f32)
-            out[...] = (resid_cols[...].astype(f32) + total).astype(bf16)
+            out[span, :] = own_share[0, span, :].astype(bf16)
         else:
-            r["z_share"][j] = own_share[j].astype(bf16)
+            r["z_share"][j, span, :] = own_share[j, span, :].astype(bf16)
             turn = jnp.where(at < z, 0, 1)
             copy = chain.copy(
-                r["z_share"].at[j],
-                r["z_got"].at[turn, at],
-                r["zs_sent"].at[j],
-                r["zs_landed"].at[turn, at],
+                r["z_share"].at[j, span, :],
+                r["z_got"].at[turn, at, span, :],
+                r["zs_sent"].at[j, p],
+                r["zs_landed"].at[turn, at, p],
                 jnp.where(at < z, z - 1, z + 1) * x_size + x,
             )
             chain.launch(copy)
 
     for j in reversed(range(z_size)):
-        send_share(j)
+        send_twins(j)
         if j + 1 < z_size:
             finish_share(j + 1)
+        send_share(j)
     finish_share(0)
     chain.finish()
-    for phase in dense_sums + hidden_gathers + row_gathers + expert_sums:
+    for copy in copies:
+        copy.wait_send()
+    for phase in [mix] + dense_sums + hidden_gathers + row_gathers + expert_sums:
         phase.finish()
 
 
+PIECES = 2
+PARTS = (2, 1, 0, 3)
+WIDE = 512
 WEIGHTS = ("dense_gate", "dense_up", "gate", "up", "down", "dense_down")
 
 
-def layer(own_cols, resid_cols, side, weights, top, ep_size, tp_size):
-    count, width = own_cols.shape
+def layer(partial, ffn_gain, route_ids, route_logits, weights, branch_gate, tokens, ep_size, tp_size):
+    count, width = tokens.shape[0], tokens.shape[1] // tp_size
+    top = route_ids.shape[0]
     bf16, f32 = jnp.bfloat16, jnp.float32
     vmem, dma = pltpu.VMEM, pltpu.SemaphoreType.DMA
     x_size = fast_extent("ep", ep_size)
@@ -877,9 +874,21 @@
     slow = tp_size // fast
     named = {name: vmem(array.shape, bf16) for name, array in zip(WEIGHTS, weights)}
     named.update(
-        load_sems=dma((len(weights),)),
+        load_sems=dma((len(weights) + 2,)),
+        tokens=vmem((count, width), bf16),
+        branch=vmem((width,), bf16),
+        own_cols=vmem((count, width), bf16),
+        side=vmem((8, 128), f32),
+        late=vmem((8, 128), f32),
+        stat=vmem((8, 128), f32),
+        stat_got=vmem((tp_size - 1, 8, 128), f32),
+        stat_sent=dma((tp_size - 1,)),
+        stat_landed=dma((tp_size - 1,)),
         cols=vmem((ep_size, count, width), bf16),
         sides=vmem((ep_size, 8, 128), f32),
+        lates=vmem((ep_size, 8, 128), f32),
+        table=vmem((ep_size, 128, 128), f32),
+        row_scale=vmem((rounds, rows, 128), f32),
         turned=vmem((ep_size, 128, 128), f32),
         hidden=vmem((rounds, rows, inner), bf16),
         expert_out=vmem((rounds, rows, width), bf16),
@@ -888,16 +897,14 @@
         x_got=vmem((z_size, x_size - 1, count, width), bf16),
         z_share=vmem((z_size, count, width), bf16),
         z_got=vmem((2, z_size, count, width), bf16),
-        z_sent=dma((2, z_size)),
-        z_landed=dma((z_size,)),
-        x_sent=dma((x_size - 1, z_size)),
-        x_landed=dma((x_size - 1, z_size)),
-        side_sent=dma((ep_size - 1,)),
-        side_landed=dma((ep_size - 1,)),
-        xs_sent=dma((ep_size,)),
-        xs_landed=dma((z_size, x_size - 1)),
-        zs_sent=dma((z_size,)),
-        zs_landed=dma((2, z_size)),
+        z_sent=dma((2, z_size, PIECES + 2)),
+        z_landed=dma((z_size, PIECES + 2)),
+        x_sent=dma((x_size - 1, z_size, PIECES + 2)),
+        x_landed=dma((x_size - 1, z_size, PIECES + 2)),
+        xs_sent=dma((ep_size, PIECES)),
+        xs_landed=dma((z_size, x_size - 1, PIECES)),
+        zs_sent=dma((z_size, PIECES)),
+        zs_landed=dma((2, z_size, PIECES)),
     )
     extra = []
     for _ in range(rounds):
@@ -911,18 +918,19 @@
         extra += reduce_scratch(fast, slow, count, 2 * hidden_width, 1)
         extra += gather_sems(fast, slow, 1) + gather_sems(fast, slow, pieces)
         extra += reduce_scratch(fast, slow, rows, width, pieces)
+    extra += reduce_scratch(fast, slow, count, width, PIECES)
     whole = pl.BlockSpec(memory_space=pltpu.VMEM)
     far = pl.BlockSpec(memory_space=pl.ANY)
     return pl.pallas_call(
         functools.partial(layer_kernel, ep_size, tp_size, top, cap, tuple(named)),
-        out_shape=jax.ShapeDtypeStruct((count, width), bf16),
-        in_specs=[whole] * 3 + [far] * len(weights),
-        out_specs=whole,
+        out_shape=(jax.ShapeDtypeStruct((count, width), bf16),) * 2,
+        in_specs=[whole] * 4 + [far] * (len(weights) + 2),
+        out_specs=(whole, whole),
         scratch_shapes=list(named.values()) + extra,
         compiler_params=pltpu.CompilerParams(
-            collective_id=1, has_side_effects=True, vmem_limit_bytes=62 << 20
+            collective_id=0, has_side_effects=True, vmem_limit_bytes=62 << 20
         ),
-    )(own_cols, resid_cols, side, *weights)
+    )(partial, ffn_gain, route_ids, route_logits, *weights, branch_gate, tokens)
 
 
 def shards(
@@ -952,7 +960,7 @@
 ):
     tp_count = lax.axis_size("tp")
     ep_count = lax.axis_size("ep")
-    reads, new_states = mixer(
+    partial, new_states = mixer(
         tokens,
         mix_gain.reshape(1, -1),
         in_proj,
@@ -965,19 +973,28 @@
         c_imag,
         skip_gain.reshape(1, -1),
         states,
+        out_proj,
     )
-    own_cols, resid_cols, side = mixer_exit(
-        reads,
-        out_proj,
-        tokens,
+    weights = (
+        dense_gate,
+        dense_up,
+        expert_gate[0],
+        expert_up[0],
+        expert_down[0],
+        dense_down,
+    )
+    gathered, resid_cols = layer(
+        partial,
         ffn_gain.reshape(1, -1),
-        branch_gate.astype(jnp.float32).reshape(1, -1),
         route_ids.T,
         route_logits.T,
+        weights,
+        branch_gate,
+        tokens,
+        ep_count,
         tp_count,
     )
-    weights = (dense_gate, dense_up, expert_gate[0], expert_up[0], expert_down[0], dense_down)
-    output = layer(own_cols, resid_cols, side, weights, route_ids.shape[1], ep_count, tp_count)
+    output = (resid_cols.astype(jnp.float32) + gathered.astype(jnp.float32)).astype(jnp.bfloat16)
     return (output, new_states)
 
 

time: 112 us -> 93.3 us (0.83)
  Pallas kernels: 108 us -> 90.5 us
  local copies, waits for them, and re-layouts: 1.62 us -> 0 us
    pallas_call x2 -> x1, Pallas kernels: 21.1 us -> 6.26 us  [mixer(): pl.pallas_call(mixer_kernel, out_shape=(jax.ShapeDtypeStruct(tokens.shape...]
    pallas_call x1, Pallas kernels: 87.2 us -> 84.2 us  [layer(): pl.pallas_call(functools.partial(layer_kernel, ep_size, tp_size, top, cap...]
    convert_element_type x0 -> x1, other arithmetic: none -> 1.75 us  [shards(): (resid_cols.astype(jnp.float32) + gathered.astype(jnp.float32)).astype(jn...]
    unnamed x1 -> x0, local copies, waits for them, and re-layouts: 1.62 us -> none
    reshape x1 -> x0, other arithmetic: 1.3 us -> none  [shards(): branch_gate.astype(jnp.float32).reshape(1, -1)]
where the time goes in v3:
time: 93.3 us; the launch traced here: 92.9 us
  Pallas kernels  90.5 us (97%)
  other arithmetic  1.75 us (2%)
    pallas_call x1, Pallas kernels, layer(): pl.pallas_call(functools.partial(layer_kernel, ep_size, tp_size, top, cap...  84.2 us
    pallas_call x1, Pallas kernels, mixer(): pl.pallas_call(mixer_kernel, out_shape=(jax.ShapeDtypeStruct(tokens.shape...  6.26 us

profile of v3, /device:TPU:0, one launch (start us, length us, event | category | flops | bytes accessed | tf_op | source)
XLA Modules:
  0.0 92.9 jit_solution(532094197099062393)
XLA Ops:
  0.6 6.3 %shard_map.230 = (bf16[96,4096]{1,0:T(8,128)(2,1)}, f32[2,96,1024]{2,1,0:T(8,128)}) custom-call(bf16[96,4096]{1,0:T(8,128)(2,1)} %refs_11_.3, f32[1,4096]{1,0:T(1,128)} %bitcast.16, bf16[4096,256]{1,0:T(8,128)(2,1)} %refs_2_.1, f32[16,64]{1,0:T(8,128)} %refs_3_.1, f32[16,64]{1,0:T(8,128)} %refs_4_.2, f32[1,16]{1,0:T(1,128)} %bitcast.21, ...), custom_call_target="tpu_custom_call" | custom-call | tf_op jit(solution)/shard_map/pallas_call | solution.py:334
  6.9 84.2 %shard_map.231 = (bf16[96,1024]{1,0:T(8,128)(2,1)}, bf16[96,1024]{1,0:T(8,128)(2,1)}) custom-call(bf16[96,4096]{1,0:T(8,128)(2,1)} %get-tuple-element.6.refs_0_, f32[1,4096]{1,0:T(1,128)} %bitcast.17, s32[2,96]{1,0:T(2,128)} %bitcast.18, f32[2,96]{1,0:T(2,128)} %bitcast.19, bf16[1024,768]{1,0:T(8,128)(2,1)} %refs_4_.3, bf16[1024,768]{1,0:T(8,128)(2,1)} %refs_5_.1, ...), custom_call_target="tpu_custom_call" | custom-call | tf_op jit(solution)/shard_map/pallas_call | solution.py:924
  91.1 1.8 %add_convert_fusion = bf16[96,1024]{1,0:T(8,128)(2,1)} fusion(bf16[96,1024]{1,0:T(8,128)(2,1)} %get-tuple-element.8, bf16[96,1024]{1,0:T(8,128)(2,1)} %get-tuple-element.7), kind=kLoop, calls=%fused_computation | loop fusion | flops 393216 | bytes 589824 | tf_op jit(solution)/shard_map/convert_element_type | solution.py:997

commit v4 on v3

--- a/solution.py
+++ b/solution.py
@@ -403,15 +403,17 @@
                 copy.wait_send()
             else:
                 pl.when(cond)(copy.wait_send)
+        self.pending = []
 
 
 def layer_kernel(ep_size, tp_size, top, cap, names, *refs):
     partial, ffn_gain, route_ids, route_logits = refs[:4]
     weights_hbm, branch_hbm, tokens_hbm = refs[4:10], refs[10], refs[11]
-    out, resid_cols, refs = refs[12], refs[13], refs[14:]
+    out, refs = refs[12], refs[13:]
     r = dict(zip(names, refs))
     extra = list(refs[len(names) :])
-    own_cols, side, late = r["own_cols"], r["side"], r["late"]
+    own_cols, resid_cols = r["own_cols"], r["resid_cols"]
+    side, late = r["side"], r["late"]
     f32, bf16 = jnp.float32, jnp.bfloat16
     chain, grid = Chain(ep_size), Grid("tp", tp_size)
     z_size, x_size, z, x = chain.z_size, chain.x_size, chain.z, chain.x
@@ -712,42 +714,43 @@
         else:
             for p in PARTS:
                 pass_on(j, p, j > 2 * fewer, False)
+        if j == end - 1:
+            for p in PARTS:
+                pass_on(end, p, fewer > 0)
         for q in range(1, x_size):
             wait_chunk(j - 1, q)
             process(j - 1, q)
         process(j, 0)
-    for p in PARTS:
-        pass_on(end, p, fewer > 0)
     for q in range(1, x_size):
         wait_chunk(end - 1, q)
         process(end - 1, q)
+    for p in PARTS:
+        pass_on(end, p, fewer == 0, False)
     for load in loads[2:5]:
         load.wait()
     for g in range(last):
         expert_hidden(g)
-    for p in PARTS:
-        pass_on(end, p, fewer == 0, False)
     process(end, 0)
+    for q in range(1, x_size):
+        wait_chunk(end, q)
+        process(end, q)
+    dense_sums[last].relay()
     for g in range(last):
         dense_hidden(g)
         expert_part(g)
         expert_sums[g].push()
-    for q in range(1, x_size):
-        wait_chunk(end, q)
-        process(end, q)
-    dense_sums[last].relay()
-    expert_sums[0].relay(range(pieces // 2))
     expert_hidden(last)
     expert_part(last)
     expert_sums[last].push()
     dense_hidden(last)
-    for g in reversed(range(1, rounds)):
+    expert_sums[last].relay()
+    for g in reversed(range(last)):
         expert_sums[g].relay()
-    expert_sums[0].relay(range(pieces // 2, pieces))
-    for g in range(rounds):
-        hidden_gathers[g].relay()
-    for g in range(rounds):
-        hidden_gathers[g].arrive()
+    for copy in copies:
+        copy.wait_send()
+    for phase in [mix] + row_gathers + dense_sums:
+        phase.finish()
+    chain.finish()
     loads[5].wait()
 
     collected, own_share = set(), r["own_share"]
@@ -757,6 +760,10 @@
         g, at = i // tp_size, i % tp_size
         chunks = tp_size // pieces
         piece = at // chunks
+        if g not in collected:
+            collected.add(g)
+            hidden_gathers[g].relay()
+            hidden_gathers[g].arrive()
         if (g, piece) not in collected:
             collected.add((g, piece))
             rows = chunks * cap
@@ -826,29 +833,39 @@
                 ].astype(f32)
 
         if j == 0:
-            out[span, :] = own_share[0, span, :].astype(bf16)
+            total = own_share[0, span, :].astype(bf16).astype(f32)
+            out[span, :] = (resid_cols[span, :].astype(f32) + total).astype(bf16)
         else:
             r["z_share"][j, span, :] = own_share[j, span, :].astype(bf16)
-            turn = jnp.where(at < z, 0, 1)
-            copy = chain.copy(
-                r["z_share"].at[j, span, :],
-                r["z_got"].at[turn, at, span, :],
-                r["zs_sent"].at[j, p],
-                r["zs_landed"].at[turn, at, p],
-                jnp.where(at < z, z - 1, z + 1) * x_size + x,
-            )
-            chain.launch(copy)
+            share_copy(j, p).start()
+
+    def share_copy(j, p):
+        at, span = chain.at(j), pl.ds(p * step, step)
+        turn = jnp.where(at < z, 0, 1)
+        return chain.copy(
+            r["z_share"].at[j, span, :],
+            r["z_got"].at[turn, at, span, :],
+            r["zs_sent"].at[j, p],
+            r["zs_landed"].at[turn, at, p],
+            jnp.where(at < z, z - 1, z + 1) * x_size + x,
+        )
+
+    def finish_if(cond, j):
+        if 0 < j < z_size:
+            pl.when(cond)(functools.partial(finish_share, j))
 
     for j in reversed(range(z_size)):
         send_twins(j)
-        if j + 1 < z_size:
-            finish_share(j + 1)
+        finish_if(fewer == 0, j + 1)
+        finish_if(fewer > 0, j + 2)
         send_share(j)
+    finish_if(fewer > 0, 1)
     finish_share(0)
+    for j in range(1, z_size):
+        for p in range(PIECES):
+            share_copy(j, p).wait_send()
     chain.finish()
-    for copy in copies:
-        copy.wait_send()
-    for phase in [mix] + dense_sums + hidden_gathers + row_gathers + expert_sums:
+    for phase in hidden_gathers + expert_sums:
         phase.finish()
 
 
@@ -878,6 +895,7 @@
         tokens=vmem((count, width), bf16),
         branch=vmem((width,), bf16),
         own_cols=vmem((count, width), bf16),
+        resid_cols=vmem((count, width), bf16),
         side=vmem((8, 128), f32),
         late=vmem((8, 128), f32),
         stat=vmem((8, 128), f32),
@@ -923,9 +941,9 @@
     far = pl.BlockSpec(memory_space=pl.ANY)
     return pl.pallas_call(
         functools.partial(layer_kernel, ep_size, tp_size, top, cap, tuple(named)),
-        out_shape=(jax.ShapeDtypeStruct((count, width), bf16),) * 2,
+        out_shape=jax.ShapeDtypeStruct((count, width), bf16),
         in_specs=[whole] * 4 + [far] * (len(weights) + 2),
-        out_specs=(whole, whole),
+        out_specs=whole,
         scratch_shapes=list(named.values()) + extra,
         compiler_params=pltpu.CompilerParams(
             collective_id=0, has_side_effects=True, vmem_limit_bytes=62 << 20
@@ -983,7 +1001,7 @@
         expert_down[0],
         dense_down,
     )
-    gathered, resid_cols = layer(
+    output = layer(
         partial,
         ffn_gain.reshape(1, -1),
         route_ids.T,
@@ -994,7 +1012,6 @@
         ep_count,
         tp_count,
     )
-    output = (resid_cols.astype(jnp.float32) + gathered.astype(jnp.float32)).astype(jnp.bfloat16)
     return (output, new_states)
 
 

time: 93.3 us -> 89.7 us (0.961)
  Pallas kernels: 90.5 us -> 87.2 us
  other arithmetic: 1.75 us -> 0 us
  local copies, waits for them, and re-layouts: 0 us -> 1.62 us
    pallas_call x1, Pallas kernels: 84.2 us -> 81 us  [layer(): pl.pallas_call(functools.partial(layer_kernel, ep_size, tp_size, top, cap...]
    convert_element_type x1 -> x0, other arithmetic: 1.75 us -> none  [shards(): (resid_cols.astype(jnp.float32) + gathered.astype(jnp.float32)).astype(jn...]
    unnamed x0 -> x1, local copies, waits for them, and re-layouts: none -> 1.62 us
where the time goes in v4:
time: 89.7 us; the launch traced here: 89.5 us
  Pallas kernels  87.2 us (97%)
  local copies, waits for them, and re-layouts  1.62 us (2%)
    pallas_call x1, Pallas kernels, layer(): pl.pallas_call(functools.partial(layer_kernel, ep_size, tp_size, top, cap...  81 us
    pallas_call x1, Pallas kernels, mixer(): pl.pallas_call(mixer_kernel, out_shape=(jax.ShapeDtypeStruct(tokens.shape...  6.27 us

profile of v4, /device:TPU:0, one launch (start us, length us, event | category | flops | bytes accessed | tf_op | source)
XLA Modules:
  0.0 89.5 jit_solution(8326600254953095992)
XLA Ops:
  0.6 6.3 %shard_map.230 = (bf16[96,4096]{1,0:T(8,128)(2,1)}, f32[2,96,1024]{2,1,0:T(8,128)}) custom-call(bf16[96,4096]{1,0:T(8,128)(2,1)} %refs_11_.3, f32[1,4096]{1,0:T(1,128)} %bitcast.16, bf16[4096,256]{1,0:T(8,128)(2,1)} %refs_2_.1, f32[16,64]{1,0:T(8,128)} %refs_3_.1, f32[16,64]{1,0:T(8,128)} %refs_4_.2, f32[1,16]{1,0:T(1,128)} %bitcast.21, ...), custom_call_target="tpu_custom_call" | custom-call | tf_op jit(solution)/shard_map/pallas_call | solution.py:334
  6.9 81.0 %shard_map.231 = bf16[96,1024]{1,0:T(8,128)(2,1)} custom-call(bf16[96,4096]{1,0:T(8,128)(2,1)} %get-tuple-element.4.refs_0_, f32[1,4096]{1,0:T(1,128)} %bitcast.17, s32[2,96]{1,0:T(2,128)} %bitcast.18, f32[2,96]{1,0:T(2,128)} %bitcast.19, bf16[1024,768]{1,0:T(8,128)(2,1)} %refs_4_.3, bf16[1024,768]{1,0:T(8,128)(2,1)} %refs_5_.1, bf16[4096,768]{1,0:T(8,128)(2,1)} %bitcast.11, ...), custom_call_target="tpu_custom_call" | custom-call | tf_op jit(solution)/shard_map/pallas_call | solution.py:942
  87.9 1.6 %copy.26 = bf16[96,1024]{1,0:T(8,128)(2,1)} copy(bf16[96,1024]{1,0:T(8,128)(2,1)} %shard_map.231) | data formatting | bytes 393216

commit v5 on v4

--- a/solution.py
+++ b/solution.py
@@ -245,9 +245,9 @@
     near, fresh, normed, sems = refs[15:28], refs[28], refs[29], refs[30]
     loads = []
     for item, (source, target) in enumerate(zip(far, near)):
-        load = pltpu.make_async_copy(source, target, sems.at[item])
-        load.start()
-        loads.append(load)
+        loads.append(pltpu.make_async_copy(source, target, sems.at[item]))
+    for item in (3, 4, 5, 0, 1, 2, 6, 7, 11, 8, 9, 10, 12):
+        loads[item].start()
     tokens, mix_gain, in_proj, decay_rate, frequency, log_step = near[:6]
     b_real, b_imag, c_real, c_imag, skip_gain, old, out_proj = near[6:]
     count, width = tokens.shape
@@ -407,11 +407,13 @@
 
 
 def layer_kernel(ep_size, tp_size, top, cap, names, *refs):
-    partial, ffn_gain, route_ids, route_logits = refs[:4]
+    early_hbm = refs[:4]
     weights_hbm, branch_hbm, tokens_hbm = refs[4:10], refs[10], refs[11]
     out, refs = refs[12], refs[13:]
     r = dict(zip(names, refs))
     extra = list(refs[len(names) :])
+    early = [r[name] for name in EARLY]
+    partial, ffn_gain, route_ids, route_logits = early
     own_cols, resid_cols = r["own_cols"], r["resid_cols"]
     side, late = r["side"], r["late"]
     f32, bf16 = jnp.float32, jnp.bfloat16
@@ -441,17 +443,6 @@
 
     mix = Reduce(grid, partial, PIECES, True, take(8))
     mine = pl.ds(pl.multiple_of(grid.me * width, 128), width)
-    near = [r[name] for name in WEIGHTS]
-    loads = []
-    transfers = list(zip(weights_hbm, near))
-    transfers.insert(0, (tokens_hbm.at[:, mine], r["tokens"]))
-    transfers.insert(1, (branch_hbm.at[mine], r["branch"]))
-    for item, (source, target) in enumerate(transfers):
-        load = pltpu.make_async_copy(source, target, r["load_sems"].at[item])
-        load.start()
-        loads.append(load)
-    first_loads, loads = loads[:2], loads[2:]
-    dense_gate, dense_up, gate, up, down, dense_down = near
     barrier = pltpu.get_barrier_semaphore()
     for k in range(1, x_size):
         pl.semaphore_signal(
@@ -469,8 +460,22 @@
         pl.semaphore_signal(
             barrier, inc=1, device_id={"tp": (grid.me + k) % tp_size}, device_id_type=MESH
         )
+    near = [r[name] for name in WEIGHTS]
+    loads = []
+    transfers = list(zip(weights_hbm, near))
+    transfers = list(zip(early_hbm, early)) + transfers
+    transfers.insert(0, (tokens_hbm.at[:, mine], r["tokens"]))
+    transfers.insert(1, (branch_hbm.at[mine], r["branch"]))
+    for item, (source, target) in enumerate(transfers):
+        load = pltpu.make_async_copy(source, target, r["load_sems"].at[item])
+        load.start()
+        loads.append(load)
+    first_loads, loads = loads[:6], loads[6:]
+    dense_gate, dense_up, gate, up, down, dense_down = near
     beside = (z + z_size - 1) // z_size + (2 * z_size - 2 - z) // z_size
     pl.semaphore_wait(barrier, x_size + tp_size - 2 + beside)
+    for load in first_loads:
+        load.wait()
     mix.push()
     logits = route_logits[...]
     raised = jnp.exp(logits - jnp.max(logits, axis=0, keepdims=True))
@@ -478,8 +483,6 @@
     late[...] = jnp.zeros((8, 128), f32)
     side[0:top, 0:count] = route_ids[...].astype(f32)
     side[top : 2 * top, 0:count] = raised / jnp.sum(raised, axis=0, keepdims=True)
-    for load in first_loads:
-        load.wait()
     mix.relay()
 
     cols, sides, lates = r["cols"], r["sides"], r["lates"]
@@ -665,12 +668,20 @@
     def expert_part(g):
         target = part[g]
 
-        @pl.loop(0, tp_size * width // wide)
-        def _(step):
-            span = pl.ds(pl.multiple_of(step * wide, 128), wide)
-            target[:, span] = jnp.dot(
-                hidden[g], down[:, span], preferred_element_type=f32
-            ).astype(bf16)
+        def block(dest):
+            @pl.loop(0, width // wide)
+            def _(step):
+                span = pl.ds(pl.multiple_of(dest * width + step * wide, 128), wide)
+                target[:, span] = jnp.dot(
+                    hidden[g], down[:, span], preferred_element_type=f32
+                ).astype(bf16)
+
+        for k in range(1, grid.slow + 1):
+            for q in range(1, grid.fast):
+                block(grid.index(k, q))
+                expert_sums[g].push_part(k, q)
+        for k in range(1, grid.slow + 1):
+            block(grid.index(k, 0))
 
     def dense_hidden(g):
         i = g * tp_size + grid.me
@@ -738,10 +749,8 @@
     for g in range(last):
         dense_hidden(g)
         expert_part(g)
-        expert_sums[g].push()
     expert_hidden(last)
     expert_part(last)
-    expert_sums[last].push()
     dense_hidden(last)
     expert_sums[last].relay()
     for g in reversed(range(last)):
@@ -872,6 +881,7 @@
 PIECES = 2
 PARTS = (2, 1, 0, 3)
 WIDE = 512
+EARLY = ("partial", "ffn_gain", "route_ids", "route_logits")
 WEIGHTS = ("dense_gate", "dense_up", "gate", "up", "down", "dense_down")
 
 
@@ -890,8 +900,10 @@
     fast = fast_extent("tp", tp_size)
     slow = tp_size // fast
     named = {name: vmem(array.shape, bf16) for name, array in zip(WEIGHTS, weights)}
+    firsts = (partial, ffn_gain, route_ids, route_logits)
+    named.update({name: vmem(array.shape, array.dtype) for name, array in zip(EARLY, firsts)})
     named.update(
-        load_sems=dma((len(weights) + 2,)),
+        load_sems=dma((len(weights) + 6,)),
         tokens=vmem((count, width), bf16),
         branch=vmem((width,), bf16),
         own_cols=vmem((count, width), bf16),
@@ -942,7 +954,7 @@
     return pl.pallas_call(
         functools.partial(layer_kernel, ep_size, tp_size, top, cap, tuple(named)),
         out_shape=jax.ShapeDtypeStruct((count, width), bf16),
-        in_specs=[whole] * 4 + [far] * (len(weights) + 2),
+        in_specs=[far] * (len(weights) + 6),
         out_specs=whole,
         scratch_shapes=list(named.values()) + extra,
         compiler_params=pltpu.CompilerParams(

time: 89.7 us -> 88.2 us (0.983)
  Pallas kernels: 87.2 us -> 85.7 us
    pallas_call x1, Pallas kernels: 81 us -> 80 us  [layer(): pl.pallas_call(functools.partial(layer_kernel, ep_size, tp_size, top, cap...]
where the time goes in v5:
time: 88.2 us; the launch traced here: 88 us
  Pallas kernels  85.7 us (97%)
  local copies, waits for them, and re-layouts  1.62 us (2%)
    pallas_call x1, Pallas kernels, layer(): pl.pallas_call(functools.partial(layer_kernel, ep_size, tp_size, top, cap...  80 us
    pallas_call x1, Pallas kernels, mixer(): pl.pallas_call(mixer_kernel, out_shape=(jax.ShapeDtypeStruct(tokens.shape...  5.69 us

profile of v5, /device:TPU:0, one launch (start us, length us, event | category | flops | bytes accessed | tf_op | source)
XLA Modules:
  0.0 88.0 jit_solution(17869247869263490069)
XLA Ops:
  0.6 5.7 %shard_map.230 = (bf16[96,4096]{1,0:T(8,128)(2,1)}, f32[2,96,1024]{2,1,0:T(8,128)}) custom-call(bf16[96,4096]{1,0:T(8,128)(2,1)} %refs_11_.3, f32[1,4096]{1,0:T(1,128)} %bitcast.16, bf16[4096,256]{1,0:T(8,128)(2,1)} %refs_2_.1, f32[16,64]{1,0:T(8,128)} %refs_3_.1, f32[16,64]{1,0:T(8,128)} %refs_4_.2, f32[1,16]{1,0:T(1,128)} %bitcast.21, ...), custom_call_target="tpu_custom_call" | custom-call | tf_op jit(solution)/shard_map/pallas_call | solution.py:334
  6.3 80.0 %shard_map.231 = bf16[96,1024]{1,0:T(8,128)(2,1)} custom-call(bf16[96,4096]{1,0:T(8,128)(2,1)} %get-tuple-element.4.refs_0_, f32[1,4096]{1,0:T(1,128)} %bitcast.17, s32[2,96]{1,0:T(2,128)} %bitcast.18, f32[2,96]{1,0:T(2,128)} %bitcast.19, bf16[1024,768]{1,0:T(8,128)(2,1)} %refs_4_.3, bf16[1024,768]{1,0:T(8,128)(2,1)} %refs_5_.1, bf16[4096,768]{1,0:T(8,128)(2,1)} %bitcast.11, ...), custom_call_target="tpu_custom_call" | custom-call | tf_op jit(solution)/shard_map/pallas_call | solution.py:954
  86.4 1.6 %copy.26 = bf16[96,1024]{1,0:T(8,128)(2,1)} copy(bf16[96,1024]{1,0:T(8,128)(2,1)} %shard_map.231) | data formatting | bytes 393216
